TPU v7x, 32 devices: a whole 2x2x4 slice. The times are simulated.
32 devices in a mesh: sp: 16 (over z, y, x), tp: 2 (over core).
Axes of the slice: x: 2, y: 2, z: 4, core: 2. Of those that a mesh axis runs over, the one named last changes fastest.
Arguments:
- tokens: bfloat16 [16384, 2048], P('sp', 'tp'), may hold values from -6 to 6
- norm_gain: float32 [2048], replicated, may hold values from 0.1 to 1.9
- w_conv_a: bfloat16 [2048, 1024], P('sp', 'tp'), may hold values from -0.125 to 0.125
- w_conv_gate: bfloat16 [2048, 1024], P('sp', 'tp'), may hold values from -0.125 to 0.125
- conv_weight: float32 [31, 1024], P(None, 'tp'), may hold values from -16 to 16
- conv_gain: float32 [1024], P('tp'), may hold values from 0.1 to 1.9
- w_query: bfloat16 [2048, 512], P('sp', 'tp'), may hold values from -0.125 to 0.125
- w_key: bfloat16 [2048, 512], P('sp', 'tp'), may hold values from -0.125 to 0.125
- w_value: bfloat16 [2048, 1024], P('sp', 'tp'), may hold values from -0.125 to 0.125
- w_outgate: bfloat16 [2048, 1024], P('sp', 'tp'), may hold values from -0.125 to 0.125
- w_decay: bfloat16 [2048, 512], P('sp', 'tp'), may hold values from -0.125 to 0.125
- decay_bias: float32 [512], P('tp'), may hold values from 0 to 12
- decay_extra: float32 [16384, 512], P('sp', 'tp'), may hold values from -2 to 0
- head_gain: float32 [128], replicated, may hold values from 0.1 to 1.9
- init_state: float32 [8, 64, 128], P('tp'), may hold values from -768 to 768
- w_out_conv: bfloat16 [1024, 2048], P('tp', 'sp'), may hold values from -0.125 to 0.125
- w_out_gla: bfloat16 [1024, 2048], P('tp', 'sp'), may hold values from -0.125 to 0.125
Outputs:
- mixed: bfloat16 [16384, 2048], P(('sp', 'tp'))
All inputs are finite; a program needn't handle non-finite values.
Results may differ from a plain program's by a relative error of at most 0.022.
Values may be sent and summed in bfloat16 or wider, within the bound.
No kernel may reach another device: no remote copies, remote signals or barrier semaphores. Data moves between devices by JAX's collectives and lax.ppermute only.
A program may use at most 128 MiB of HBM per device.

v0:
```python
import functools

import jax
import jax.numpy as jnp
from jax import lax
from jax.experimental import pallas as pl
from jax.experimental.pallas import tpu as pltpu
from jax.sharding import PartitionSpec as P


HK = 64
HV = 128
BLOCK = 128
LANES = 128
HALO = 32
ROW_TILE = 256
DIRECT = 16


epsilon = 1e-06
gate_divisor = 16.0
f32 = jnp.float32
bf16 = jnp.bfloat16
SMEM = pl.BlockSpec(memory_space=pltpu.SMEM)


def whole(shape):
    return pl.BlockSpec(shape, lambda i: (0,) * len(shape))


def params(megabytes):
    return pltpu.CompilerParams(
        dimension_semantics=("arbitrary",), vmem_limit_bytes=megabytes * 1024 * 1024
    )


def dot(a, b):
    return jnp.dot(a, b, preferred_element_type=f32)


def flip(value, axis, mask):
    count = lax.axis_size(axis)
    pairs = [(i, i ^ mask) for i in range(count)]
    return lax.ppermute(value, axis, pairs)


def is_middle(place):
    return (place >> 2 ^ place >> 3) & 1


def exchange(value, axis):
    count = lax.axis_size(axis)
    pairs = [(i, i ^ 12) for i in range(count) if is_middle(i)]
    return lax.ppermute(value, axis, pairs)


def hand_on(value, axis):
    count = lax.axis_size(axis)
    pairs = [(i, i ^ 4) for i in range(count) if is_middle(i)]
    return lax.ppermute(value, axis, pairs)


def chosen(axis, dim, *options):
    flag = is_middle(lax.axis_index(axis)).astype(jnp.int32).reshape(1)
    return choose(flag, options, dim)


def relayed(own, axis, dim):
    def send(value, mask):
        return flip(value, axis, mask)

    na = exchange(own, axis)
    z1 = send(own, 4)
    x0 = send(own, 1)
    y0 = send(own, 2)
    fa = hand_on(na, axis)
    nb = exchange(z1, axis)
    x1 = send(z1, 1)
    y1 = send(z1, 2)
    d0 = send(y0, 1)
    a0 = chosen(axis, dim, (na, fa))
    fb = hand_on(nb, axis)
    xa = send(a0, 1)
    ya = send(a0, 2)
    d1 = send(x1, 2)
    b0 = chosen(axis, dim, (nb, fb))
    xb = send(b0, 1)
    yb = send(b0, 2)
    da = send(ya, 1)
    db = send(xb, 2)
    order = [own, x0, y0, d0, z1, x1, y1, d1] + [None] * 8 + [a0, xa, ya, da, b0, xb, yb, db]
    return [(piece, (place,)) for place, piece in enumerate(order) if piece is not None]


def doubled(own, axis, dim, turn):
    first, second = (2, 1) if turn else (1, 2)

    def send(value, mask):
        return flip(value, axis, mask)

    z1 = send(own, 4)
    na = exchange(own, axis)
    nb = exchange(z1, axis)
    fa = hand_on(na, axis)
    fb = hand_on(nb, axis)
    x0 = send(own, first)
    pair = chosen(axis, dim, (own, own), (z1, z1))
    far = chosen(axis, dim, (na, fa), (nb, fb))
    yp = send(pair, second)
    x1 = send(x0, 4)
    dp = send(yp, first)
    xq = send(far, first)
    yq = send(far, second)
    dq = send(xq, second)

    def nears(place):
        return (place, place | 4)

    def fars(place):
        return (16 + place, 20 + place)

    return [
        (pair, nears(0)),
        (x0, (first,)),
        (x1, (first | 4,)),
        (yp, nears(second)),
        (dp, nears(3)),
        (far, fars(0)),
        (xq, fars(first)),
        (yq, fars(second)),
        (dq, fars(3)),
    ]


def spread(own, axis, dim, turn, plan):
    count = lax.axis_size(axis)
    if count == DIRECT:
        if plan == "single":
            return relayed(own, axis, dim)
        return doubled(own, axis, dim, turn)
    pieces = {0: own}
    mask = 1
    while mask < count:
        for place in list(pieces):
            pieces[place | mask] = flip(pieces[place], axis, mask)
        mask *= 2
    return [(piece, (place,)) for place, piece in pieces.items()]


def gathered(own, axis, dim, turn, plan):
    count = lax.axis_size(axis)
    if count > DIRECT or count & (count - 1):
        pieces = [(lax.all_gather(own, axis, axis=dim, tiled=True), (0,))]
        offs = jnp.zeros((1,), jnp.int32)
    else:
        pieces = spread(own, axis, dim, turn, plan)
        place = lax.axis_index(axis)
        order = jnp.arange(count, dtype=jnp.int32)
        turned = 4 * is_middle(place)
        near = jnp.arange(4, dtype=jnp.int32)
        order = jnp.concatenate([order, near ^ 8 ^ turned, near ^ 12 ^ turned])
        offs = (order ^ place) * own.shape[dim]
    return [p for p, _ in pieces], tuple(q for _, q in pieces), offs


def shifted(value, axis, steps):
    count = lax.axis_size(axis)
    return lax.ppermute(value, axis, [(i, i + steps) for i in range(count - steps)])


def entering(held, packed, axis):
    place = lax.axis_index(axis)
    bits = lax.axis_size(axis).bit_length() - 1
    for bit in range(bits):
        upper = ((place >> bit) & 1).astype(jnp.int32).reshape(1)
        received = flip(packed, axis, 1 << bit)
        if bit + 1 == bits:
            return held, received, upper
        held, packed = combine(upper, received, held)


def choose_body(flag, *refs, dim):
    out, sem = refs[-2:]
    ins = refs[:-2]
    for number, middle in enumerate((True, False)):
        picked = [pair[number] for pair in zip(ins[::2], ins[1::2])]

        @pl.when((flag[0] == 1) == middle)
        def _():
            copies = []
            start = 0
            for k, ref in enumerate(picked):
                there = pl.ds(start, ref.shape[dim])
                target = out.at[:, there] if dim else out.at[there, :]
                copies.append(pltpu.make_async_copy(ref, target, sem.at[k]))
                start += ref.shape[dim]
            for copy in copies:
                copy.start()
            for copy in copies:
                copy.wait()


def choose(flag, options, dim):
    shape = list(options[0][0].shape)
    shape[dim] = sum(first.shape[dim] for first, _ in options)
    flat = [array for pair in options for array in pair]
    vmem = pl.BlockSpec(memory_space=pltpu.VMEM)
    return pl.pallas_call(
        functools.partial(choose_body, dim=dim),
        in_specs=[SMEM] + [vmem] * len(flat),
        out_specs=vmem,
        out_shape=jax.ShapeDtypeStruct(tuple(shape), flat[0].dtype),
        scratch_shapes=[pltpu.SemaphoreType.DMA((len(options),))],
        compiler_params=pltpu.CompilerParams(vmem_limit_bytes=2 * 1024 * 1024),
        name="choose",
    )(flag, *flat)


def norm_body(places, *refs):
    *ins, gain, out = refs
    total = None
    for ref in ins:
        wide = ref[...].astype(f32)
        part = jnp.sum(wide * wide, axis=1, keepdims=True)
        total = part if total is None else total + part
    scale = lax.rsqrt(total / out.shape[1] + epsilon)
    for k, ref in enumerate(ins):
        cols = pl.ds(pl.multiple_of(places[k], LANES), ref.shape[1])
        out[:, cols] = (ref[...].astype(f32) * scale * gain[0:1, cols]).astype(bf16)


def normalize(parts, places, gain):
    rows, total = parts[0].shape[0], gain.shape[0]
    tile = min(ROW_TILE, rows)
    return pl.pallas_call(
        norm_body,
        grid=(rows // tile,),
        in_specs=[SMEM]
        + [pl.BlockSpec((tile, p.shape[1]), lambda i: (i, 0)) for p in parts]
        + [whole((1, total))],
        out_specs=pl.BlockSpec((tile, total), lambda i: (i, 0)),
        out_shape=jax.ShapeDtypeStruct((rows, total), bf16),
        compiler_params=params(58),
        name="normalize",
    )(places, *parts, gain[None, :])


def place_pieces(offs, refs, weight, places, dim):
    for ref, spots in zip(refs, places):
        size = ref.shape[dim] // len(spots)
        for k, spot in enumerate(spots):
            there = pl.ds(pl.multiple_of(offs[spot], size), size)
            here = slice(k * size, (k + 1) * size)
            if dim:
                weight[:, there] = ref[:, here]
            else:
                weight[there, :] = ref[here, :]


def project_body(offs, normed, *refs, places):
    weight = refs[-1]
    outs = refs[len(places) : -1]

    @pl.when(pl.program_id(0) == 0)
    def _():
        place_pieces(offs, refs, weight, places, 0)

    start = 0
    for out in outs:
        width = out.shape[1]
        out[...] = dot(normed[...], weight[:, start : start + width]).astype(out.dtype)
        start += width


def project(normed, pieces, places, offs, widths, kinds):
    rows, depth = normed.shape
    total = sum(widths)
    tile = min(ROW_TILE, rows)
    return pl.pallas_call(
        functools.partial(project_body, places=places),
        grid=(rows // tile,),
        in_specs=[SMEM, pl.BlockSpec((tile, depth), lambda i: (i, 0))]
        + [whole(p.shape) for p in pieces],
        out_specs=[pl.BlockSpec((tile, w), lambda i: (i, 0)) for w in widths],
        out_shape=[jax.ShapeDtypeStruct((rows, w), k) for w, k in zip(widths, kinds)],
        scratch_shapes=[pltpu.VMEM((depth, total), bf16)],
        compiler_params=params(58),
        cost_estimate=pl.CostEstimate(
            flops=2 * rows * depth * total, bytes_accessed=rows * depth * 2, transcendentals=0
        ),
        name="project",
    )(offs, normed, *pieces)


def conv_project_body(offs, normed, before, *refs, places):
    weight = refs[-1]
    gated, gate_out, rim = refs[len(places) : -1]
    width = gated.shape[1]

    def gate(values):
        left = values[:, :width].astype(bf16).astype(f32)
        right = values[:, width : 2 * width].astype(bf16).astype(f32)
        return (left * jax.nn.sigmoid(right)).astype(bf16)

    @pl.when(pl.program_id(0) == 0)
    def _():
        place_pieces(offs, refs, weight, places, 0)
        rim[...] = gate(dot(before[...], weight[:, : 2 * width]))

    gated[...] = gate(dot(normed[...], weight[:, : 2 * width]))
    gate_out[...] = dot(normed[...], weight[:, 2 * width :]).astype(bf16)


def conv_project(normed, before, pieces, places, offs, width, gate_width):
    rows, depth = normed.shape
    total = 2 * width + gate_width
    tile = min(ROW_TILE, rows)
    return pl.pallas_call(
        functools.partial(conv_project_body, places=places),
        grid=(rows // tile,),
        in_specs=[SMEM, pl.BlockSpec((tile, depth), lambda i: (i, 0)), whole(before.shape)]
        + [whole(p.shape) for p in pieces],
        out_specs=[
            pl.BlockSpec((tile, width), lambda i: (i, 0)),
            pl.BlockSpec((tile, gate_width), lambda i: (i, 0)),
            whole((before.shape[0], width)),
        ],
        out_shape=[
            jax.ShapeDtypeStruct((rows, width), bf16),
            jax.ShapeDtypeStruct((rows, gate_width), bf16),
            jax.ShapeDtypeStruct((before.shape[0], width), bf16),
        ],
        scratch_shapes=[pltpu.VMEM((depth, total), bf16)],
        compiler_params=params(58),
        cost_estimate=pl.CostEstimate(
            flops=2 * rows * depth * total, bytes_accessed=rows * depth * 2, transcendentals=0
        ),
        name="conv_project",
    )(offs, normed, before, *pieces)


def conv_body(gated, rim, taps, out, sums, extended):
    rows, width = gated.shape
    count = taps.shape[0]
    first = HALO - count + 1
    chunk = 64
    extended[:HALO] = rim[...].astype(f32)
    extended[HALO : HALO + rows] = gated[...].astype(f32)
    extended[HALO + rows :] = jnp.zeros((8, width), f32)

    def step(i, carry):
        base = pl.multiple_of(i * chunk, chunk)
        there = pl.ds(base, chunk)
        total = jnp.zeros((chunk, LANES), f32)
        square = jnp.zeros((chunk, LANES), f32)
        for lane in range(0, width, LANES):
            here = slice(lane, lane + LANES)
            near = extended[pl.ds(base, chunk + HALO + 8), here]
            result = None
            for residue in range(8):
                acc = None
                for start in range(0, HALO + 1, 8):
                    tap = start + residue - first
                    if 0 <= tap < count:
                        part = taps[tap : tap + 1, here] * near[start : start + chunk + 8]
                        acc = part if acc is None else acc + part
                if residue:
                    acc = pltpu.roll(acc, chunk + 8 - residue, 0)
                acc = acc[:chunk]
                result = acc if result is None else result + acc
            out[there, here] = result.astype(bf16)
            total = total + result
            square = square + result * result
        sums[there, 0:1] = jnp.sum(total, axis=1, keepdims=True)
        sums[there, 1:2] = jnp.sum(square, axis=1, keepdims=True)
        return carry

    lax.fori_loop(0, rows // chunk, step, 0)


def convolve(gated, rim, taps):
    rows, width = gated.shape
    return pl.pallas_call(
        conv_body,
        out_shape=[
            jax.ShapeDtypeStruct((rows, width), bf16),
            jax.ShapeDtypeStruct((rows, 2), f32),
        ],
        scratch_shapes=[
            pltpu.VMEM((HALO + rows + 8, width), f32),
        ],
        compiler_params=pltpu.CompilerParams(vmem_limit_bytes=58 * 1024 * 1024),
        cost_estimate=pl.CostEstimate(
            flops=20 * rows * width * taps.shape[0], bytes_accessed=rows * width * 6, transcendentals=0
        ),
        name="convolve",
    )(gated, rim, taps)


def gla_body(query, keys, values, pre, bias, extra, local, since, held, packed, state, prefix):
    rows, channels = query.shape
    step = pl.program_id(0)
    group = min(2, channels // HK)
    kw, vw = HK * group, HV * group

    @pl.when(step == 0)
    def _():
        state[...] = jnp.zeros(state.shape, f32)
        prefix[...] = jnp.zeros(prefix.shape, f32)

    biased = pre[...] + bias[...]
    log_decay = (jnp.minimum(biased, 0.0) - jnp.log1p(jnp.exp(-jnp.abs(biased)))) / gate_divisor
    log_decay = log_decay + extra[...]
    at = lax.broadcasted_iota(jnp.int32, (rows, rows), 0)
    by = lax.broadcasted_iota(jnp.int32, (rows, rows), 1)
    causal = at >= by
    cum = jnp.dot(
        causal.astype(f32), log_decay, preferred_element_type=f32, precision=lax.Precision.HIGHEST
    )
    middle = cum[rows // 2 - 1 : rows // 2]
    end = cum[rows - 1 : rows]
    before = prefix[0:1]
    q = query[...].astype(f32) * HK ** (-0.5)
    k = keys[...].astype(f32)
    grown = jnp.exp(cum)
    q_mid = q * jnp.exp(cum - middle)
    k_mid = (k * jnp.exp(middle - cum)).astype(bf16)
    k_end = (k * jnp.exp(end - cum)).astype(bf16)
    q_run = q * grown
    since[...] = (q_run * jnp.exp(before)).astype(bf16)
    q_run = q_run.astype(bf16)
    end_decay = jnp.exp(end)
    key_row = lax.broadcasted_iota(jnp.int32, (kw, kw), 0)
    key_col = lax.broadcasted_iota(jnp.int32, (kw, kw), 1)
    lane = lax.broadcasted_iota(jnp.int32, (rows, kw), 1)
    own_head = (
        lax.broadcasted_iota(jnp.int32, (kw, vw), 0) // HK
        == lax.broadcasted_iota(jnp.int32, (kw, vw), 1) // HV
    )
    for p in range(channels // kw):
        ks = slice(p * kw, (p + 1) * kw)
        v = values[:, p * vw : (p + 1) * vw]
        s = state[p]
        carried = dot(q_run[:, ks], s.astype(bf16))
        for h in range(group):
            q_head = jnp.where(lane // HK == h, q_mid[:, ks], 0.0).astype(bf16)
            scores = lax.dot_general(
                q_head, k_mid[:, ks], (((1,), (1,)), ((), ())), preferred_element_type=f32
            )
            scores = jnp.where(causal, scores, 0.0).astype(bf16)
            hs = slice(h * HV, (h + 1) * HV)
            first = p * vw + h * HV
            local[:, first : first + HV] = (dot(scores, v[:, hs]) + carried[:, hs]).astype(bf16)
        column = jnp.sum(jnp.where(key_row == key_col, end_decay[:, ks], 0.0), axis=1, keepdims=True)
        added = lax.dot_general(
            k_end[:, ks], v, (((0,), (0,)), ((), ())), preferred_element_type=f32
        )
        state[p] = s * column + jnp.where(own_head, added, 0.0)
    prefix[0:1] = before + end

    @pl.when(step == pl.num_programs(0) - 1)
    def _():
        everything = prefix[0:1]
        for p in range(channels // kw):
            column = jnp.sum(
                jnp.where(key_row == key_col, everything[:, p * kw : (p + 1) * kw], 0.0), axis=1, keepdims=True
            )
            held[p * kw : (p + 1) * kw, 3 * HV :] = jnp.broadcast_to(column, (kw, HV))
            for h in range(group):
                row = p * kw + h * HK
                own = state[p, h * HK : (h + 1) * HK, h * HV : (h + 1) * HV]
                held[row : row + HK, 2 * HV : 3 * HV] = own
        held[:, : 2 * HV] = jnp.zeros((channels, 2 * HV), f32)
        packed[:, :HV], packed[:, HV:] = packing(held[:, 2 * HV : 3 * HV], held[:, 3 * HV :])


def linear_attention(query, keys, values, pre, bias, extra):
    rows, channels = query.shape
    wide = values.shape[1]
    group = min(2, channels // HK)
    tile = min(BLOCK, rows)
    narrow = pl.BlockSpec((tile, channels), lambda i: (i, 0))
    broad = pl.BlockSpec((tile, wide), lambda i: (i, 0))
    return pl.pallas_call(
        gla_body,
        grid=(rows // tile,),
        in_specs=[narrow, narrow, broad, narrow, whole((1, channels)), narrow],
        out_specs=[broad, narrow, whole((channels, 4 * HV)), whole((channels, 2 * HV))],
        out_shape=[
            jax.ShapeDtypeStruct((rows, wide), bf16),
            jax.ShapeDtypeStruct((rows, channels), bf16),
            jax.ShapeDtypeStruct((channels, 4 * HV), f32),
            jax.ShapeDtypeStruct((channels, 2 * HV), bf16),
        ],
        scratch_shapes=[
            pltpu.VMEM((channels // HK // group, HK * group, HV * group), f32),
            pltpu.VMEM((8, channels), f32),
        ],
        compiler_params=params(24),
        cost_estimate=pl.CostEstimate(
            flops=20 * rows * tile * wide, bytes_accessed=rows * wide * 8, transcendentals=0
        ),
        name="linear_attention",
    )(query, keys, values, pre, bias, extra)


def packing(state, logs):
    high = logs.astype(bf16)
    lane = lax.broadcasted_iota(jnp.int32, logs.shape, 1)
    low = (logs - high.astype(f32)).astype(bf16)
    return state.astype(bf16), jnp.where(lane < HV // 2, high.astype(f32), low.astype(f32)).astype(bf16)


def unpacking(packed):
    half = packed[:, HV : 2 * HV].astype(f32)
    logs = half[:, 0:1] + half[:, HV // 2 : HV // 2 + 1]
    return packed[:, :HV].astype(f32), jnp.broadcast_to(logs, half.shape)


def combine_body(upper, packed, held, held_out, packed_out):
    state, logs = unpacking(packed)
    above = upper[0] == 1
    pre, pre_logs, own, own_logs = (held[:, k * HV : (k + 1) * HV] for k in range(4))
    held_out[:, :HV] = jnp.where(above, jnp.exp(pre_logs) * state + pre, pre)
    held_out[:, HV : 2 * HV] = jnp.where(above, pre_logs + logs, pre_logs)
    joined = jnp.where(above, jnp.exp(own_logs) * state + own, jnp.exp(logs) * own + state)
    joined_logs = own_logs + logs
    held_out[:, 2 * HV : 3 * HV] = joined
    held_out[:, 3 * HV :] = joined_logs
    packed_out[:, :HV], packed_out[:, HV:] = packing(joined, joined_logs)


def combine(upper, packed, held):
    vmem = pl.BlockSpec(memory_space=pltpu.VMEM)
    return pl.pallas_call(
        combine_body,
        in_specs=[SMEM, vmem, vmem],
        out_specs=[vmem, vmem],
        out_shape=[
            jax.ShapeDtypeStruct(held.shape, f32),
            jax.ShapeDtypeStruct(packed.shape, bf16),
        ],
        compiler_params=pltpu.CompilerParams(vmem_limit_bytes=4 * 1024 * 1024),
        name="combine",
    )(upper, packed, held)


def finish_body(start, offs, *refs, channels, parts, places):
    sums, refs = refs[:parts], refs[parts:]
    conv, conv_gain, local, since, upper, packed, held, init, gate, head_gain, *refs = refs
    weights, (out, state, act) = refs[: len(places)], refs[len(places) :]

    @pl.when(pl.program_id(0) == 0)
    def _():
        last, logs = unpacking(packed)
        above = upper[0] == 1
        pre, pre_logs = held[:, :HV], held[:, HV : 2 * HV]
        started = jnp.where(above, jnp.exp(pre_logs) * last + pre, pre)
        logs = jnp.where(above, pre_logs + logs, pre_logs)
        state[...] = (started + jnp.exp(logs) * init[...]).astype(bf16)

    width = conv.shape[1]
    stats = sums[0][...]
    for more in sums[1:]:
        stats = stats + more[...]
    mean_val = stats[:, 0:1] / channels
    square_mean = stats[:, 1:2] / channels
    normal = (conv[...].astype(f32) - mean_val) * lax.rsqrt(square_mean - mean_val * mean_val + epsilon)
    normal = normal * conv_gain[...]
    act[:, :width] = (normal * jax.nn.sigmoid(normal)).astype(bf16)
    keys = since.shape[1]
    group = min(2, keys // HK)
    kw = HK * group
    lane = lax.broadcasted_iota(jnp.int32, (since.shape[0], kw), 1)
    for head in range(keys // HK):
        p, h = divmod(head, group)
        q = jnp.where(lane // HK == h, since[:, p * kw : (p + 1) * kw].astype(f32), 0.0).astype(bf16)
        hs = slice(head * HV, (head + 1) * HV)
        attn = local[:, hs].astype(f32) + dot(q, state[p * kw : (p + 1) * kw])
        attn = attn * lax.rsqrt(jnp.mean(attn * attn, axis=1, keepdims=True) + epsilon)
        gated = gate[:, hs].astype(f32)
        gated = gated * jax.nn.sigmoid(gated)
        act[:, width + head * HV : width + (head + 1) * HV] = (attn * head_gain[...] * gated).astype(bf16)
    for ref, spots in zip(weights, places):
        size = ref.shape[1] // len(spots)
        values = dot(act[...], ref[...]).astype(bf16)
        for k, spot in enumerate(spots):
            there = pl.ds(pl.multiple_of(offs[spot], size), size)
            out[:, there] = values[:, k * size : (k + 1) * size]


def finish(first, rows, sums, conv, conv_gain, local, since, before, init, gate, head_gain, out_weights, total, channels):
    pieces, places, offs = out_weights
    width, wide = conv.shape[1], local.shape[1]
    tile = min(ROW_TILE, rows)
    held, packed, upper = before
    start = (first // tile).astype(jnp.int32).reshape(1)

    def tiled(cols):
        return pl.BlockSpec((tile, cols), lambda i, at: (at[0] + i, 0))

    def fixed(shape):
        return pl.BlockSpec(shape, lambda i, at: (0, 0))

    spec = pltpu.PrefetchScalarGridSpec(
        num_scalar_prefetch=1,
        grid=(rows // tile,),
        in_specs=[SMEM]
        + [tiled(2) for _ in sums]
        + [
            tiled(width),
            fixed((1, width)),
            tiled(wide),
            tiled(since.shape[1]),
            SMEM,
            fixed(packed.shape),
            fixed(held.shape),
            fixed(init.shape),
            tiled(wide),
            fixed((1, HV)),
        ]
        + [pl.BlockSpec(memory_space=pltpu.VMEM) for _ in pieces],
        out_specs=pl.BlockSpec((tile, total), lambda i, at: (i, 0)),
        scratch_shapes=[pltpu.VMEM(init.shape, bf16), pltpu.VMEM((tile, width + wide), bf16)],
    )
    return pl.pallas_call(
        functools.partial(finish_body, channels=channels, parts=len(sums), places=places),
        grid_spec=spec,
        out_shape=jax.ShapeDtypeStruct((rows, total), bf16),
        compiler_params=params(56),
        cost_estimate=pl.CostEstimate(
            flops=2 * rows * (width + wide) * total, bytes_accessed=rows * total * 2, transcendentals=0
        ),
        name="finish",
    )(start, offs, *sums, conv, conv_gain, local, since, upper, packed, held, init, gate, head_gain, *pieces)


def normed_rows(own, axis, norm_gain):
    if lax.axis_size(axis) != 2:
        full = lax.all_gather(own, axis, axis=1, tiled=True)
        return normalize([full], jnp.zeros((1,), jnp.int32), norm_gain)
    other = flip(own, axis, 1)
    mine = lax.axis_index(axis)
    places = jnp.stack([mine, 1 - mine]).astype(jnp.int32) * own.shape[1]
    return normalize([own, other], places, norm_gain)


def per_device(
    tokens,
    norm_gain,
    w_conv_a,
    w_conv_gate,
    conv_weight,
    conv_gain,
    w_query,
    w_key,
    w_value,
    w_outgate,
    w_decay,
    decay_bias,
    decay_extra,
    head_gain,
    init_state,
    w_out_conv,
    w_out_gla,
):
    rows = tokens.shape[0]
    groups = lax.axis_size("tp")
    width = w_conv_a.shape[1]
    channels = w_query.shape[1]
    wide = w_value.shape[1]

    gla_own = jnp.concatenate([w_query, w_key, w_value, w_decay], axis=1)
    conv_own = jnp.concatenate([w_conv_a, w_conv_gate, w_outgate], axis=1)
    out_own = jnp.concatenate([w_out_conv, w_out_gla], axis=0)
    gla_weights = gathered(gla_own, "sp", 0, 0, "single")
    conv_weights = gathered(conv_own, "sp", 0, 0, "double")
    out_weights = gathered(out_own, "sp", 1, 1, "double")

    rim = shifted(tokens[rows - HALO :], "sp", 1)
    normed = normed_rows(tokens, "tp", norm_gain)
    normed_rim = normed_rows(rim, "tp", norm_gain)

    query, keys, values, decay_pre = project(
        normed, *gla_weights, (channels, channels, wide, channels), (bf16, bf16, bf16, f32)
    )
    local, since, *end = linear_attention(
        query, keys, values, decay_pre, decay_bias[None, :], decay_extra
    )
    before = entering(*end, "sp")

    gated, gate, gated_rim = conv_project(normed, normed_rim, *conv_weights, width, wide)
    conv, sums = convolve(gated, gated_rim, conv_weight)
    sums = [sums, flip(sums, "tp", 1)] if groups == 2 else [lax.psum(sums, "tp")]

    init = init_state.reshape(channels, HV)
    total = norm_gain.shape[0]

    def rows_from(first, count):
        return finish(
            jnp.asarray(first),
            count,
            sums,
            conv,
            conv_gain[None, :],
            local,
            since,
            before,
            init,
            gate,
            head_gain[None, :],
            out_weights,
            total,
            width * groups,
        )

    if groups != 2:
        return lax.psum_scatter(rows_from(0, rows), "tp", scatter_dimension=0, tiled=True)
    half = rows // 2
    mine = lax.axis_index("tp")
    received = flip(rows_from((1 - mine) * half, half), "tp", 1)
    kept = rows_from(mine * half, half)
    return (kept.astype(f32) + received.astype(f32)).astype(bf16)


def solution(mesh):
    placed = (
        P("sp", "tp"),
        P(),
        P("sp", "tp"),
        P("sp", "tp"),
        P(None, "tp"),
        P("tp"),
        P("sp", "tp"),
        P("sp", "tp"),
        P("sp", "tp"),
        P("sp", "tp"),
        P("sp", "tp"),
        P("tp"),
        P("sp", "tp"),
        P(),
        P("tp", None, None),
        P("tp", "sp"),
        P("tp", "sp"),
    )

    return jax.shard_map(
        per_device, mesh=mesh, in_specs=placed, out_specs=P(("sp", "tp"), None), check_vma=False
    )
```

profile of v0, /device:TPU:0, one launch (start us, length us, event | category | flops | bytes accessed | tf_op | source)
XLA Modules:
  0.0 228.6 jit_solution(6718519994641722979)
XLA Ops:
  3.9 2.6 %collective-permute-start.19 = (bf16[128,1280]{1,0:T(8,128)(2,1)S(1)}, bf16[128,1280]{1,0:T(8,128)(2,1)S(1)}, u32[]{:S(2)}, u32[]{:S(2)}) collective-permute-start(bf16[128,1280]{1,0:T(8,128)(2,1)S(1)} %constant_dynamic-update-slice_fusion.3.refs_0_), channel_id=1, source_target_pairs={{0,8},{2,10},{4,12},{6,14},{8,0},{10,2},{12,4},{14,6},{16,24},{18,... | collective-permute-start | bytes 983048 | tf_op jit(solution)/shard_map/ppermute | solution.py:44
  8.0 3.4 %collective-permute-start.1 = (bf16[32,1024]{1,0:T(8,128)(2,1)S(1)}, bf16[32,1024]{1,0:T(8,128)(2,1)S(1)}, u32[]{:S(2)}, u32[]{:S(2)}) collective-permute-start(bf16[32,1024]{1,0:T(8,128)(2,1)S(1)} %slice.3), channel_id=1, source_target_pairs={{0,2},{2,4},{4,6},{6,8},{8,10},{10,12},{12,14},{14,16},{16,18},{18... | collective-permute-start | bytes 196616 | tf_op jit(solution)/shard_map/ppermute | solution.py:168
  13.3 4.4 %collective-permute-start.37 = (bf16[1024,128]{1,0:T(8,128)(2,1)S(1)}, bf16[1024,128]{1,0:T(8,128)(2,1)S(1)}, u32[]{:S(2)}, u32[]{:S(2)}) collective-permute-start(bf16[1024,128]{1,0:T(8,128)(2,1)S(1)} %constant_dynamic-update-slice_fusion.7.refs_0_.refs_1_), channel_id=1, source_target_pairs={{0,8},{2,10},{4,12},{6,14},{8,0},{10,2},{12,4},{14,6},{16,24},{18,... | collective-permute-start | bytes 786440 | tf_op jit(solution)/shard_map/ppermute | solution.py:44
  20.0 1.5 collective-permute-start.17
  22.4 1.4 collective-permute-done.37.refs_2_.refs_3_
  23.9 1.7 collective-permute-start.3
  25.6 1.5 collective-permute-start.16
  27.8 2.2 collective-permute-done.17.refs_2_
  30.0 1.4 collective-permute-start.28
  31.3 2.5 %collective-permute-done.16.refs_1_ = bf16[128,1280]{1,0:T(8,128)(2,1)} collective-permute-done((bf16[128,1280]{1,0:T(8,128)(2,1)S(1)}, bf16[128,1280]{1,0:T(8,128)(2,1)}, u32[]{:S(2)}, u32[]{:S(2)}) %collective-permute-start.16) | collective-permute-done | bytes 327712 | tf_op jit(solution)/shard_map/ppermute | solution.py:44
  33.9 1.3 collective-permute-start.24
  35.2 1.6 collective-permute-start.20
  38.1 8.0 %collective-permute-done.24.refs_1_ = bf16[128,1280]{1,0:T(8,128)(2,1)S(1)} collective-permute-done((bf16[128,1280]{1,0:T(8,128)(2,1)S(1)}, bf16[128,1280]{1,0:T(8,128)(2,1)S(1)}, u32[]{:S(2)}, u32[]{:S(2)}) %collective-permute-start.24) | collective-permute-done | bytes 327712 | tf_op jit(solution)/shard_map/ppermute | solution.py:60
  48.2 1.3 collective-permute-start.9
  49.6 1.3 collective-permute-start.11
  52.7 7.2 %collective-permute-done.29.refs_1_ = bf16[128,1280]{1,0:T(8,128)(2,1)} collective-permute-done((bf16[128,1280]{1,0:T(8,128)(2,1)}, bf16[128,1280]{1,0:T(8,128)(2,1)}, u32[]{:S(2)}, u32[]{:S(2)}) %collective-permute-start.29) | collective-permute-done | bytes 327712 | tf_op jit(solution)/shard_map/ppermute | solution.py:60
  60.2 1.9 choose.9.refs_12_
  63.1 5.2 %collective-permute-done.9.refs_1_ = bf16[128,1536]{1,0:T(8,128)(2,1)S(1)} collective-permute-done((bf16[128,1536]{1,0:T(8,128)(2,1)S(1)}, bf16[128,1536]{1,0:T(8,128)(2,1)S(1)}, u32[]{:S(2)}, u32[]{:S(2)}) %collective-permute-start.9) | collective-permute-done | bytes 393248 | tf_op jit(solution)/shard_map/ppermute | solution.py:60
  70.2 3.8 %collective-permute-done.11.refs_3_ = bf16[128,1536]{1,0:T(8,128)(2,1)S(1)} collective-permute-done((bf16[128,1536]{1,0:T(8,128)(2,1)S(1)}, bf16[128,1536]{1,0:T(8,128)(2,1)S(1)}, u32[]{:S(2)}, u32[]{:S(2)}) %collective-permute-start.11) | collective-permute-done | bytes 393248 | tf_op jit(solution)/shard_map/ppermute | solution.py:60
  75.8 1.5 collective-permute-start.32
  80.0 6.0 %normalize.2.normed = bf16[1024,2048]{1,0:T(8,128)(2,1)} custom-call(s32[2]{0:T(128)} %add_multiply_fusion.places, bf16[1024,1024]{1,0:T(8,128)(2,1)} %refs_0_.1, bf16[1024,1024]{1,0:T(8,128)(2,1)} %collective-permute-done.refs_1_, f32[1,2048]{1,0:T(1,128)} %bitcast.17), custom_call_target="tpu_custom_call" | custom-call | tf_op jit(solution)/shard_map/normalize/pallas_call | solution.py:235
  86.0 1.5 collective-permute-start.4
  87.4 1.4 collective-permute-start.42
  90.8 3.2 %collective-permute-done.32.refs_15_ = bf16[128,1280]{1,0:T(8,128)(2,1)} collective-permute-done((bf16[128,1280]{1,0:T(8,128)(2,1)}, bf16[128,1280]{1,0:T(8,128)(2,1)}, u32[]{:S(2)}, u32[]{:S(2)}) %collective-permute-start.32) | collective-permute-done | bytes 327712 | tf_op jit(solution)/shard_map/ppermute | solution.py:44
  94.1 1.6 collective-permute-start.12
  95.7 10.3 %project.1 = (bf16[1024,256]{1,0:T(8,128)(2,1)}, bf16[1024,256]{1,0:T(8,128)(2,1)}, bf16[1024,512]{1,0:T(8,128)(2,1)}, f32[1024,256]{1,0:T(8,128)}) custom-call(s32[24]{0:T(128)} %fusion.offs, bf16[1024,2048]{1,0:T(8,128)(2,1)} %normalize.2.normed, bf16[128,1280]{1,0:T(8,128)(2,1)} %copy-done.31, bf16[128,1280]{1,0:T(8,128)(2,1)} %collective-permute-done.16.refs_1_, ...), custom_call_target="tpu_custom_call" | custom-call | flops 5368709120 | bytes 4194304 | tf_op jit(solution)/shard_map/project/pallas_call | solution.py:279
  110.5 9.2 %linear_attention.1 = (bf16[1024,512]{1,0:T(8,128)(2,1)S(1)}, bf16[1024,256]{1,0:T(8,128)(2,1)S(1)}, f32[256,512]{1,0:T(8,128)S(1)}, bf16[256,256]{1,0:T(8,128)(2,1)S(1)}) custom-call(bf16[1024,256]{1,0:T(8,128)(2,1)S(1)} %copy-done.19, bf16[1024,256]{1,0:T(8,128)(2,1)S(1)} %copy-done.20, bf16[1024,512]{1,0:T(8,128)(2,1)S(1)} %copy-done.17, ...), custom_call_target="tpu_custom_call" | custom-call | flops 1342177280 | bytes 4194304 | tf_op jit(solution)/shard_map/linear_attention/pallas_call | solution.py:484
  120.2 1.4 collective-permute-start.44
  121.6 1.3 collective-permute-start.43
  123.0 3.2 %collective-permute-done.33.packed = bf16[256,256]{1,0:T(8,128)(2,1)S(1)} collective-permute-done((bf16[256,256]{1,0:T(8,128)(2,1)S(1)}, bf16[256,256]{1,0:T(8,128)(2,1)S(1)}, u32[]{:S(2)}, u32[]{:S(2)}) %collective-permute-start.33) | collective-permute-done | bytes 131104 | tf_op jit(solution)/shard_map/ppermute | solution.py:44
  126.9 4.9 %collective-permute-done.43.refs_1_ = bf16[1024,128]{1,0:T(8,128)(2,1)} collective-permute-done((bf16[1024,128]{1,0:T(8,128)(2,1)}, bf16[1024,128]{1,0:T(8,128)(2,1)}, u32[]{:S(2)}, u32[]{:S(2)}) %collective-permute-start.43) | collective-permute-done | bytes 262176 | tf_op jit(solution)/shard_map/ppermute | solution.py:60
  131.7 1.3 collective-permute-start.45
  133.2 2.8 %collective-permute-start.7 = (bf16[256,1536]{1,0:T(8,128)(2,1)}, bf16[256,1536]{1,0:T(8,128)(2,1)}, u32[]{:S(2)}, u32[]{:S(2)}) collective-permute-start(bf16[256,1536]{1,0:T(8,128)(2,1)} %collective-permute-done.6.refs_3_), channel_id=1, source_target_pairs={{0,2},{2,0},{4,6},{6,4},{8,10},{10,8},{12,14},{14,12},{16,18},{18,... | collective-permute-start | bytes 2359304 | tf_op jit(solution)/shard_map/ppermute | solution.py:44
  136.0 1.9 collective-permute-start.14
  138.1 2.2 collective-permute-done.45.refs_3_
  140.9 1.4 choose.11.refs_17_
  142.4 3.4 %collective-permute-done.35.packed = bf16[256,256]{1,0:T(8,128)(2,1)S(1)} collective-permute-done((bf16[256,256]{1,0:T(8,128)(2,1)S(1)}, bf16[256,256]{1,0:T(8,128)(2,1)S(1)}, u32[]{:S(2)}, u32[]{:S(2)}) %collective-permute-start.35) | collective-permute-done | bytes 131104 | tf_op jit(solution)/shard_map/ppermute | solution.py:44
  146.0 1.7 normalize.3.before
  148.7 6.2 %collective-permute-done.5.refs_2_ = bf16[128,1536]{1,0:T(8,128)(2,1)} collective-permute-done((bf16[128,1536]{1,0:T(8,128)(2,1)}, bf16[128,1536]{1,0:T(8,128)(2,1)}, u32[]{:S(2)}, u32[]{:S(2)}) %collective-permute-start.5) | collective-permute-done | bytes 393248 | tf_op jit(solution)/shard_map/ppermute | solution.py:44
  155.2 23.3 %collective-permute-done.46.refs_18_ = bf16[1024,256]{1,0:T(8,128)(2,1)S(1)} collective-permute-done((bf16[1024,256]{1,0:T(8,128)(2,1)S(1)}, bf16[1024,256]{1,0:T(8,128)(2,1)S(1)}, u32[]{:S(2)}, u32[]{:S(2)}) %collective-permute-start.46) | collective-permute-done | bytes 524320 | tf_op jit(solution)/shard_map/ppermute | solution.py:44
  179.2 1.5 collective-permute-start.48
  180.6 1.6 collective-permute-start.36
  182.2 12.6 %conv_project.1 = (bf16[1024,512]{1,0:T(8,128)(2,1)}, bf16[1024,512]{1,0:T(8,128)(2,1)}, bf16[32,512]{1,0:T(8,128)(2,1)}) custom-call(s32[24]{0:T(128)} %fusion.offs, bf16[1024,2048]{1,0:T(8,128)(2,1)} %normalize.2.normed, bf16[32,2048]{1,0:T(8,128)(2,1)} %normalize.3.before, bf16[256,1536]{1,0:T(8,128)(2,1)} %copy-done.5, ...), custom_call_target="tpu_custom_call" | custom-call | flops 6442450944 | bytes 4194304 | tf_op jit(solution)/shard_map/conv_project/pallas_call | solution.py:318
  194.9 10.0 %convolve.1 = (bf16[1024,512]{1,0:T(8,128)(2,1)}, f32[1024,2]{1,0:T(8,128)}) custom-call(bf16[1024,512]{1,0:T(8,128)(2,1)} %get-tuple-element.24.gated, bf16[32,512]{1,0:T(8,128)(2,1)} %get-tuple-element.25.rim, f32[31,512]{1,0:T(8,128)} %taps.1), custom_call_target="tpu_custom_call" | custom-call | flops 325058560 | bytes 3145728 | tf_op jit(solution)/shard_map/convolve/pallas_call | solution.py:383
  205.7 2.1 collective-permute-done.15.refs_1_
  208.6 8.1 %finish.3 = bf16[512,2048]{1,0:T(8,128)(2,1)} custom-call(s32[1]{0:T(128)} %bitcast.13.start, s32[24]{0:T(128)} %fusion.offs, f32[1024,2]{1,0:T(8,128)} %get-tuple-element.26.refs_0_, f32[1024,2]{1,0:T(8,128)} %copy-done.24, bf16[1024,512]{1,0:T(8,128)(2,1)} %get-tuple-element.27.refs_2_, f32[1,512]{1,0:T(1,128)} %bitcast.19, bf16[1024,512]{1,0:T(8,128)(2,1)} %copy-done.2, ...), custom_call_target="tpu_custom_call" | custom-call | flops 2147483648 | bytes 2097152 | tf_op jit(solution)/shard_map/finish/pallas_call | solution.py:626
  216.8 8.1 %finish.2 = bf16[512,2048]{1,0:T(8,128)(2,1)} custom-call(s32[1]{0:T(128)} %bitcast.start, s32[24]{0:T(128)} %fusion.offs, f32[1024,2]{1,0:T(8,128)} %get-tuple-element.26.refs_0_, f32[1024,2]{1,0:T(8,128)} %copy-done.24, bf16[1024,512]{1,0:T(8,128)(2,1)} %get-tuple-element.27.refs_2_, f32[1,512]{1,0:T(1,128)} %bitcast.20, bf16[1024,512]{1,0:T(8,128)(2,1)} %copy-done.2, ...), custom_call_target="tpu_custom_call" | custom-call | flops 2147483648 | bytes 2097152 | tf_op jit(solution)/shard_map/finish/pallas_call | solution.py:626
  225.0 3.7 %add_convert_fusion = bf16[512,2048]{1,0:T(8,128)(2,1)} fusion(bf16[512,2048]{1,0:T(8,128)(2,1)S(1)} %collective-permute-done.49, bf16[512,2048]{1,0:T(8,128)(2,1)} %finish.2), kind=kLoop, calls=%fused_computation | loop fusion | flops 4194304 | bytes 6291456 | tf_op jit(solution)/shard_map/convert_element_type | solution.py:723
  (158 shorter events, 36.7 us)
Async XLA Ops:
  0.0 75.8 %collective-permute-start = (bf16[1024,1024]{1,0:T(8,128)(2,1)}, bf16[1024,1024]{1,0:T(8,128)(2,1)}, u32[]{:S(2)}, u32[]{:S(2)}) collective-permute-start(bf16[1024,1024]{1,0:T(8,128)(2,1)} %refs_0_.1), channel_id=1, source_target_pairs={{0,1},{1,0},{2,3},{3,2},{4,5},{5,4},{6,7},{7,6},{8,9},{9,8},{10,11... | collective-permute-start | bytes 6291464 | tf_op jit(solution)/shard_map/ppermute | solution.py:44
  3.9 21.7 %collective-permute-start.19 = (bf16[128,1280]{1,0:T(8,128)(2,1)S(1)}, bf16[128,1280]{1,0:T(8,128)(2,1)S(1)}, u32[]{:S(2)}, u32[]{:S(2)}) collective-permute-start(bf16[128,1280]{1,0:T(8,128)(2,1)S(1)} %constant_dynamic-update-slice_fusion.3.refs_0_), channel_id=1, source_target_pairs={{0,8},{2,10},{4,12},{6,14},{8,0},{10,2},{12,4},{14,6},{16,24},{18,... | collective-permute-start | bytes 983048 | tf_op jit(solution)/shard_map/ppermute | solution.py:44
  6.5 20.6 %collective-permute-start.23 = (bf16[128,1280]{1,0:T(8,128)(2,1)S(1)}, bf16[128,1280]{1,0:T(8,128)(2,1)S(1)}, u32[]{:S(2)}, u32[]{:S(2)}) collective-permute-start(bf16[128,1280]{1,0:T(8,128)(2,1)S(1)} %constant_dynamic-update-slice_fusion.3.refs_0_), channel_id=1, source_target_pairs={{8,16},{10,18},{12,20},{14,22},{16,8},{18,10},{20,12},{22,14},{9,1... | collective-permute-start | bytes 983048 | tf_op jit(solution)/shard_map/ppermute | solution.py:54
  8.0 10.6 %collective-permute-start.1 = (bf16[32,1024]{1,0:T(8,128)(2,1)S(1)}, bf16[32,1024]{1,0:T(8,128)(2,1)S(1)}, u32[]{:S(2)}, u32[]{:S(2)}) collective-permute-start(bf16[32,1024]{1,0:T(8,128)(2,1)S(1)} %slice.3), channel_id=1, source_target_pairs={{0,2},{2,4},{4,6},{6,8},{8,10},{10,12},{12,14},{14,16},{16,18},{18... | collective-permute-start | bytes 196616 | tf_op jit(solution)/shard_map/ppermute | solution.py:168
  13.3 10.6 %collective-permute-start.37 = (bf16[1024,128]{1,0:T(8,128)(2,1)S(1)}, bf16[1024,128]{1,0:T(8,128)(2,1)S(1)}, u32[]{:S(2)}, u32[]{:S(2)}) collective-permute-start(bf16[1024,128]{1,0:T(8,128)(2,1)S(1)} %constant_dynamic-update-slice_fusion.7.refs_0_.refs_1_), channel_id=1, source_target_pairs={{0,8},{2,10},{4,12},{6,14},{8,0},{10,2},{12,4},{14,6},{16,24},{18,... | collective-permute-start | bytes 786440 | tf_op jit(solution)/shard_map/ppermute | solution.py:44
  20.0 10.0 %collective-permute-start.17 = (bf16[128,1280]{1,0:T(8,128)(2,1)S(1)}, bf16[128,1280]{1,0:T(8,128)(2,1)}, u32[]{:S(2)}, u32[]{:S(2)}) collective-permute-start(bf16[128,1280]{1,0:T(8,128)(2,1)S(1)} %constant_dynamic-update-slice_fusion.3.refs_0_), channel_id=1, source_target_pairs={{0,4},{2,6},{4,0},{6,2},{8,12},{10,14},{12,8},{14,10},{16,20},{18,... | collective-permute-start | bytes 983048 | tf_op jit(solution)/shard_map/ppermute | solution.py:44
  23.9 11.3 %collective-permute-start.3 = (bf16[128,1536]{1,0:T(8,128)(2,1)S(1)}, bf16[128,1536]{1,0:T(8,128)(2,1)S(1)}, u32[]{:S(2)}, u32[]{:S(2)}) collective-permute-start(bf16[128,1536]{1,0:T(8,128)(2,1)S(1)} %constant_dynamic-update-slice_fusion.refs_0_.refs_1_), channel_id=1, source_target_pairs={{0,8},{2,10},{4,12},{6,14},{8,0},{10,2},{12,4},{14,6},{16,24},{18,... | collective-permute-start | bytes 1179656 | tf_op jit(solution)/shard_map/ppermute | solution.py:44
  25.6 8.3 %collective-permute-start.16 = (bf16[128,1280]{1,0:T(8,128)(2,1)S(1)}, bf16[128,1280]{1,0:T(8,128)(2,1)}, u32[]{:S(2)}, u32[]{:S(2)}) collective-permute-start(bf16[128,1280]{1,0:T(8,128)(2,1)S(1)} %constant_dynamic-update-slice_fusion.3.refs_0_), channel_id=1, source_target_pairs={{0,2},{2,0},{4,6},{6,4},{8,10},{10,8},{12,14},{14,12},{16,18},{18,... | collective-permute-start | bytes 983048 | tf_op jit(solution)/shard_map/ppermute | solution.py:44
  27.1 9.6 %collective-permute-start.8 = (bf16[128,1536]{1,0:T(8,128)(2,1)S(1)}, bf16[128,1536]{1,0:T(8,128)(2,1)S(1)}, u32[]{:S(2)}, u32[]{:S(2)}) collective-permute-start(bf16[128,1536]{1,0:T(8,128)(2,1)S(1)} %constant_dynamic-update-slice_fusion.refs_0_.refs_1_), channel_id=1, source_target_pairs={{8,16},{10,18},{12,20},{14,22},{16,8},{18,10},{20,12},{22,14},{9,1... | collective-permute-start | bytes 1179656 | tf_op jit(solution)/shard_map/ppermute | solution.py:54
  30.0 7.4 %collective-permute-start.28 = (bf16[128,1280]{1,0:T(8,128)(2,1)S(1)}, bf16[128,1280]{1,0:T(8,128)(2,1)}, u32[]{:S(2)}, u32[]{:S(2)}) collective-permute-start(bf16[128,1280]{1,0:T(8,128)(2,1)S(1)} %collective-permute-done.19.refs_4_), channel_id=1, source_target_pairs={{8,16},{10,18},{12,20},{14,22},{16,8},{18,10},{20,12},{22,14},{9,1... | collective-permute-start | bytes 983048 | tf_op jit(solution)/shard_map/ppermute | solution.py:54
  33.9 12.2 %collective-permute-start.24 = (bf16[128,1280]{1,0:T(8,128)(2,1)S(1)}, bf16[128,1280]{1,0:T(8,128)(2,1)S(1)}, u32[]{:S(2)}, u32[]{:S(2)}) collective-permute-start(bf16[128,1280]{1,0:T(8,128)(2,1)S(1)} %collective-permute-done.23.refs_0_), channel_id=1, source_target_pairs={{8,0},{10,2},{12,4},{14,6},{16,24},{18,26},{20,28},{22,30},{9,1},{... | collective-permute-start | bytes 983048 | tf_op jit(solution)/shard_map/ppermute | solution.py:60
  35.2 13.0 %collective-permute-start.20 = (bf16[128,1280]{1,0:T(8,128)(2,1)S(1)}, bf16[128,1280]{1,0:T(8,128)(2,1)}, u32[]{:S(2)}, u32[]{:S(2)}) collective-permute-start(bf16[128,1280]{1,0:T(8,128)(2,1)S(1)} %collective-permute-done.19.refs_4_), channel_id=1, source_target_pairs={{0,2},{2,0},{4,6},{6,4},{8,10},{10,8},{12,14},{14,12},{16,18},{18,... | collective-permute-start | bytes 983048 | tf_op jit(solution)/shard_map/ppermute | solution.py:44
  36.7 12.8 %collective-permute-start.10 = (bf16[128,1536]{1,0:T(8,128)(2,1)S(1)}, bf16[128,1536]{1,0:T(8,128)(2,1)S(1)}, u32[]{:S(2)}, u32[]{:S(2)}) collective-permute-start(bf16[128,1536]{1,0:T(8,128)(2,1)S(1)} %collective-permute-done.3.refs_2_.refs_3_), channel_id=1, source_target_pairs={{8,16},{10,18},{12,20},{14,22},{16,8},{18,10},{20,12},{22,14},{9,1... | collective-permute-start | bytes 1179656 | tf_op jit(solution)/shard_map/ppermute | solution.py:54
  37.4 10.8 %collective-permute-start.21 = (bf16[128,1280]{1,0:T(8,128)(2,1)S(1)}, bf16[128,1280]{1,0:T(8,128)(2,1)S(1)}, u32[]{:S(2)}, u32[]{:S(2)}) collective-permute-start(bf16[128,1280]{1,0:T(8,128)(2,1)S(1)} %collective-permute-done.19.refs_4_), channel_id=1, source_target_pairs={{0,4},{2,6},{4,0},{6,2},{8,12},{10,14},{12,8},{14,10},{16,20},{18,... | collective-permute-start | bytes 983048 | tf_op jit(solution)/shard_map/ppermute | solution.py:44
  46.8 13.1 %collective-permute-start.29 = (bf16[128,1280]{1,0:T(8,128)(2,1)}, bf16[128,1280]{1,0:T(8,128)(2,1)}, u32[]{:S(2)}, u32[]{:S(2)}) collective-permute-start(bf16[128,1280]{1,0:T(8,128)(2,1)} %collective-permute-done.28.refs_0_), channel_id=1, source_target_pairs={{8,0},{10,2},{12,4},{14,6},{16,24},{18,26},{20,28},{22,30},{9,1},{... | collective-permute-start | bytes 983048 | tf_op jit(solution)/shard_map/ppermute | solution.py:60
  48.1 14.0 %collective-permute-start.18 = (bf16[128,1280]{1,0:T(8,128)(2,1)}, bf16[128,1280]{1,0:T(8,128)(2,1)}, u32[]{:S(2)}, u32[]{:S(2)}) collective-permute-start(bf16[128,1280]{1,0:T(8,128)(2,1)} %collective-permute-done.17.refs_2_), channel_id=1, source_target_pairs={{0,2},{2,0},{4,6},{6,4},{8,10},{10,8},{12,14},{14,12},{16,18},{18,... | collective-permute-start | bytes 983048 | tf_op jit(solution)/shard_map/ppermute | solution.py:44
  48.2 20.0 %collective-permute-start.9 = (bf16[128,1536]{1,0:T(8,128)(2,1)S(1)}, bf16[128,1536]{1,0:T(8,128)(2,1)S(1)}, u32[]{:S(2)}, u32[]{:S(2)}) collective-permute-start(bf16[128,1536]{1,0:T(8,128)(2,1)S(1)} %collective-permute-done.8.refs_0_), channel_id=1, source_target_pairs={{8,0},{10,2},{12,4},{14,6},{16,24},{18,26},{20,28},{22,30},{9,1},{... | collective-permute-start | bytes 1179656 | tf_op jit(solution)/shard_map/ppermute | solution.py:60
  49.6 24.4 %collective-permute-start.11 = (bf16[128,1536]{1,0:T(8,128)(2,1)S(1)}, bf16[128,1536]{1,0:T(8,128)(2,1)S(1)}, u32[]{:S(2)}, u32[]{:S(2)}) collective-permute-start(bf16[128,1536]{1,0:T(8,128)(2,1)S(1)} %collective-permute-done.10.refs_2_), channel_id=1, source_target_pairs={{8,0},{10,2},{12,4},{14,6},{16,24},{18,26},{20,28},{22,30},{9,1},{... | collective-permute-start | bytes 1179656 | tf_op jit(solution)/shard_map/ppermute | solution.py:60
  59.9 10.2 %collective-permute-start.26 = (bf16[128,1280]{1,0:T(8,128)(2,1)}, bf16[128,1280]{1,0:T(8,128)(2,1)}, u32[]{:S(2)}, u32[]{:S(2)}) collective-permute-start(bf16[128,1280]{1,0:T(8,128)(2,1)} %choose.8.refs_8_), channel_id=1, source_target_pairs={{0,4},{2,6},{4,0},{6,2},{8,12},{10,14},{12,8},{14,10},{16,20},{18,... | collective-permute-start | bytes 983048 | tf_op jit(solution)/shard_map/ppermute | solution.py:44
  62.1 13.4 %collective-permute-start.30 = (bf16[128,1280]{1,0:T(8,128)(2,1)}, bf16[128,1280]{1,0:T(8,128)(2,1)}, u32[]{:S(2)}, u32[]{:S(2)}) collective-permute-start(bf16[128,1280]{1,0:T(8,128)(2,1)} %choose.9.refs_12_), channel_id=1, source_target_pairs={{0,2},{2,0},{4,6},{6,4},{8,10},{10,8},{12,14},{14,12},{16,18},{18,... | collective-permute-start | bytes 983048 | tf_op jit(solution)/shard_map/ppermute | solution.py:44
  69.0 17.0 %collective-permute-start.25 = (bf16[128,1280]{1,0:T(8,128)(2,1)}, bf16[128,1280]{1,0:T(8,128)(2,1)S(1)}, u32[]{:S(2)}, u32[]{:S(2)}) collective-permute-start(bf16[128,1280]{1,0:T(8,128)(2,1)} %choose.8.refs_8_), channel_id=1, source_target_pairs={{0,2},{2,0},{4,6},{6,4},{8,10},{10,8},{12,14},{14,12},{16,18},{18,... | collective-permute-start | bytes 983048 | tf_op jit(solution)/shard_map/ppermute | solution.py:44
  70.2 17.3 %collective-permute-start.22 = (bf16[128,1280]{1,0:T(8,128)(2,1)}, bf16[128,1280]{1,0:T(8,128)(2,1)S(1)}, u32[]{:S(2)}, u32[]{:S(2)}) collective-permute-start(bf16[128,1280]{1,0:T(8,128)(2,1)} %collective-permute-done.20.refs_5_), channel_id=1, source_target_pairs={{0,4},{2,6},{4,0},{6,2},{8,12},{10,14},{12,8},{14,10},{16,20},{18,... | collective-permute-start | bytes 983048 | tf_op jit(solution)/shard_map/ppermute | solution.py:44
  74.7 14.1 %collective-permute-start.31 = (bf16[128,1280]{1,0:T(8,128)(2,1)}, bf16[128,1280]{1,0:T(8,128)(2,1)S(1)}, u32[]{:S(2)}, u32[]{:S(2)}) collective-permute-start(bf16[128,1280]{1,0:T(8,128)(2,1)} %choose.9.refs_12_), channel_id=1, source_target_pairs={{0,4},{2,6},{4,0},{6,2},{8,12},{10,14},{12,8},{14,10},{16,20},{18,... | collective-permute-start | bytes 983048 | tf_op jit(solution)/shard_map/ppermute | solution.py:44
  75.5 14.1 %collective-permute-start.27 = (bf16[128,1280]{1,0:T(8,128)(2,1)}, bf16[128,1280]{1,0:T(8,128)(2,1)}, u32[]{:S(2)}, u32[]{:S(2)}) collective-permute-start(bf16[128,1280]{1,0:T(8,128)(2,1)} %collective-permute-done.26.refs_10_), channel_id=1, source_target_pairs={{0,2},{2,0},{4,6},{6,4},{8,10},{10,8},{12,14},{14,12},{16,18},{18,... | collective-permute-start | bytes 983048 | tf_op jit(solution)/shard_map/ppermute | solution.py:44
  75.8 18.3 %collective-permute-start.32 = (bf16[128,1280]{1,0:T(8,128)(2,1)}, bf16[128,1280]{1,0:T(8,128)(2,1)}, u32[]{:S(2)}, u32[]{:S(2)}) collective-permute-start(bf16[128,1280]{1,0:T(8,128)(2,1)} %collective-permute-done.30.refs_13_), channel_id=1, source_target_pairs={{0,4},{2,6},{4,0},{6,2},{8,12},{10,14},{12,8},{14,10},{16,20},{18,... | collective-permute-start | bytes 983048 | tf_op jit(solution)/shard_map/ppermute | solution.py:44
  86.0 35.6 %collective-permute-start.4 = (bf16[128,1536]{1,0:T(8,128)(2,1)S(1)}, bf16[128,1536]{1,0:T(8,128)(2,1)}, u32[]{:S(2)}, u32[]{:S(2)}) collective-permute-start(bf16[128,1536]{1,0:T(8,128)(2,1)S(1)} %constant_dynamic-update-slice_fusion.refs_0_.refs_1_), channel_id=1, source_target_pairs={{0,2},{2,0},{4,6},{6,4},{8,10},{10,8},{12,14},{14,12},{16,18},{18,... | collective-permute-start | bytes 1179656 | tf_op jit(solution)/shard_map/ppermute | solution.py:44
  87.4 32.3 %collective-permute-start.42 = (bf16[1024,128]{1,0:T(8,128)(2,1)S(1)}, bf16[1024,128]{1,0:T(8,128)(2,1)}, u32[]{:S(2)}, u32[]{:S(2)}) collective-permute-start(bf16[1024,128]{1,0:T(8,128)(2,1)S(1)} %constant_dynamic-update-slice_fusion.7.refs_0_.refs_1_), channel_id=1, source_target_pairs={{8,16},{10,18},{12,20},{14,22},{16,8},{18,10},{20,12},{22,14},{9,1... | collective-permute-start | bytes 786440 | tf_op jit(solution)/shard_map/ppermute | solution.py:54
  88.8 31.4 %collective-permute-start.38 = (bf16[1024,128]{1,0:T(8,128)(2,1)S(1)}, bf16[1024,128]{1,0:T(8,128)(2,1)S(1)}, u32[]{:S(2)}, u32[]{:S(2)}) collective-permute-start(bf16[1024,128]{1,0:T(8,128)(2,1)S(1)} %constant_dynamic-update-slice_fusion.7.refs_0_.refs_1_), channel_id=1, source_target_pairs={{0,4},{2,6},{4,0},{6,2},{8,12},{10,14},{12,8},{14,10},{16,20},{18,... | collective-permute-start | bytes 786440 | tf_op jit(solution)/shard_map/ppermute | solution.py:44
  89.7 43.4 %collective-permute-start.6 = (bf16[256,1536]{1,0:T(8,128)(2,1)S(1)}, bf16[256,1536]{1,0:T(8,128)(2,1)}, u32[]{:S(2)}, u32[]{:S(2)}) collective-permute-start(bf16[256,1536]{1,0:T(8,128)(2,1)S(1)} %choose.6.refs_0_), channel_id=1, source_target_pairs={{0,4},{2,6},{4,0},{6,2},{8,12},{10,14},{12,8},{14,10},{16,20},{18,... | collective-permute-start | bytes 2359304 | tf_op jit(solution)/shard_map/ppermute | solution.py:44
  94.1 39.1 %collective-permute-start.12 = (bf16[256,1536]{1,0:T(8,128)(2,1)S(1)}, bf16[256,1536]{1,0:T(8,128)(2,1)}, u32[]{:S(2)}, u32[]{:S(2)}) collective-permute-start(bf16[256,1536]{1,0:T(8,128)(2,1)S(1)} %choose.7.refs_5_), channel_id=1, source_target_pairs={{0,2},{2,0},{4,6},{6,4},{8,10},{10,8},{12,14},{14,12},{16,18},{18,... | collective-permute-start | bytes 2359304 | tf_op jit(solution)/shard_map/ppermute | solution.py:44
  119.7 6.4 %collective-permute-start.33 = (bf16[256,256]{1,0:T(8,128)(2,1)S(1)}, bf16[256,256]{1,0:T(8,128)(2,1)S(1)}, u32[]{:S(2)}, u32[]{:S(2)}) collective-permute-start(bf16[256,256]{1,0:T(8,128)(2,1)S(1)} %get-tuple-element.34), channel_id=1, source_target_pairs={{0,2},{2,0},{4,6},{6,4},{8,10},{10,8},{12,14},{14,12},{16,18},{18,... | collective-permute-start | bytes 393224 | tf_op jit(solution)/shard_map/ppermute | solution.py:44
  120.2 6.6 %collective-permute-start.44 = (bf16[1024,128]{1,0:T(8,128)(2,1)S(1)}, bf16[1024,128]{1,0:T(8,128)(2,1)}, u32[]{:S(2)}, u32[]{:S(2)}) collective-permute-start(bf16[1024,128]{1,0:T(8,128)(2,1)S(1)} %collective-permute-done.37.refs_2_.refs_3_), channel_id=1, source_target_pairs={{8,16},{10,18},{12,20},{14,22},{16,8},{18,10},{20,12},{22,14},{9,1... | collective-permute-start | bytes 786440 | tf_op jit(solution)/shard_map/ppermute | solution.py:54
  121.6 10.2 %collective-permute-start.43 = (bf16[1024,128]{1,0:T(8,128)(2,1)}, bf16[1024,128]{1,0:T(8,128)(2,1)}, u32[]{:S(2)}, u32[]{:S(2)}) collective-permute-start(bf16[1024,128]{1,0:T(8,128)(2,1)} %collective-permute-done.42.refs_0_), channel_id=1, source_target_pairs={{8,0},{10,2},{12,4},{14,6},{16,24},{18,26},{20,28},{22,30},{9,1},{... | collective-permute-start | bytes 786440 | tf_op jit(solution)/shard_map/ppermute | solution.py:60
  126.2 16.1 %collective-permute-start.40 = (bf16[1024,256]{1,0:T(8,128)(2,1)S(1)}, bf16[1024,256]{1,0:T(8,128)(2,1)}, u32[]{:S(2)}, u32[]{:S(2)}) collective-permute-start(bf16[1024,256]{1,0:T(8,128)(2,1)S(1)} %choose.10.refs_12_), channel_id=1, source_target_pairs={{0,2},{2,0},{4,6},{6,4},{8,10},{10,8},{12,14},{14,12},{16,18},{18,... | collective-permute-start | bytes 1572872 | tf_op jit(solution)/shard_map/ppermute | solution.py:44
  126.8 9.2 %collective-permute-start.34 = (bf16[256,256]{1,0:T(8,128)(2,1)S(1)}, bf16[256,256]{1,0:T(8,128)(2,1)S(1)}, u32[]{:S(2)}, u32[]{:S(2)}) collective-permute-start(bf16[256,256]{1,0:T(8,128)(2,1)S(1)} %get-tuple-element.36), channel_id=1, source_target_pairs={{0,4},{2,6},{4,0},{6,2},{8,12},{10,14},{12,8},{14,10},{16,20},{18,... | collective-permute-start | bytes 393224 | tf_op jit(solution)/shard_map/ppermute | solution.py:44
  131.7 8.6 %collective-permute-start.45 = (bf16[1024,128]{1,0:T(8,128)(2,1)}, bf16[1024,128]{1,0:T(8,128)(2,1)S(1)}, u32[]{:S(2)}, u32[]{:S(2)}) collective-permute-start(bf16[1024,128]{1,0:T(8,128)(2,1)} %collective-permute-done.44.refs_2_), channel_id=1, source_target_pairs={{8,0},{10,2},{12,4},{14,6},{16,24},{18,26},{20,28},{22,30},{9,1},{... | collective-permute-start | bytes 786440 | tf_op jit(solution)/shard_map/ppermute | solution.py:60
  133.1 45.5 %collective-permute-start.13 = (bf16[256,1536]{1,0:T(8,128)(2,1)S(1)}, bf16[256,1536]{1,0:T(8,128)(2,1)}, u32[]{:S(2)}, u32[]{:S(2)}) collective-permute-start(bf16[256,1536]{1,0:T(8,128)(2,1)S(1)} %choose.7.refs_5_), channel_id=1, source_target_pairs={{0,4},{2,6},{4,0},{6,2},{8,12},{10,14},{12,8},{14,10},{16,20},{18,... | collective-permute-start | bytes 2359304 | tf_op jit(solution)/shard_map/ppermute | solution.py:44
  133.2 46.0 %collective-permute-start.7 = (bf16[256,1536]{1,0:T(8,128)(2,1)}, bf16[256,1536]{1,0:T(8,128)(2,1)}, u32[]{:S(2)}, u32[]{:S(2)}) collective-permute-start(bf16[256,1536]{1,0:T(8,128)(2,1)} %collective-permute-done.6.refs_3_), channel_id=1, source_target_pairs={{0,2},{2,0},{4,6},{6,4},{8,10},{10,8},{12,14},{14,12},{16,18},{18,... | collective-permute-start | bytes 2359304 | tf_op jit(solution)/shard_map/ppermute | solution.py:44
  136.0 44.7 %collective-permute-start.14 = (bf16[256,1536]{1,0:T(8,128)(2,1)}, bf16[256,1536]{1,0:T(8,128)(2,1)}, u32[]{:S(2)}, u32[]{:S(2)}) collective-permute-start(bf16[256,1536]{1,0:T(8,128)(2,1)} %collective-permute-done.12.refs_6_), channel_id=1, source_target_pairs={{0,4},{2,6},{4,0},{6,2},{8,12},{10,14},{12,8},{14,10},{16,20},{18,... | collective-permute-start | bytes 2359304 | tf_op jit(solution)/shard_map/ppermute | solution.py:44
  140.3 5.5 %collective-permute-start.35 = (bf16[256,256]{1,0:T(8,128)(2,1)S(1)}, bf16[256,256]{1,0:T(8,128)(2,1)S(1)}, u32[]{:S(2)}, u32[]{:S(2)}) collective-permute-start(bf16[256,256]{1,0:T(8,128)(2,1)S(1)} %get-tuple-element.38), channel_id=1, source_target_pairs={{0,8},{2,10},{4,12},{6,14},{8,0},{10,2},{12,4},{14,6},{16,24},{18,... | collective-permute-start | bytes 393224 | tf_op jit(solution)/shard_map/ppermute | solution.py:44
  142.3 36.2 %collective-permute-start.46 = (bf16[1024,256]{1,0:T(8,128)(2,1)S(1)}, bf16[1024,256]{1,0:T(8,128)(2,1)S(1)}, u32[]{:S(2)}, u32[]{:S(2)}) collective-permute-start(bf16[1024,256]{1,0:T(8,128)(2,1)S(1)} %choose.11.refs_17_), channel_id=1, source_target_pairs={{0,4},{2,6},{4,0},{6,2},{8,12},{10,14},{12,8},{14,10},{16,20},{18,... | collective-permute-start | bytes 1572872 | tf_op jit(solution)/shard_map/ppermute | solution.py:44
  145.8 9.1 %collective-permute-start.5 = (bf16[128,1536]{1,0:T(8,128)(2,1)}, bf16[128,1536]{1,0:T(8,128)(2,1)}, u32[]{:S(2)}, u32[]{:S(2)}) collective-permute-start(bf16[128,1536]{1,0:T(8,128)(2,1)} %collective-permute-done.4.refs_1_), channel_id=1, source_target_pairs={{0,8},{2,10},{4,12},{6,14},{8,0},{10,2},{12,4},{14,6},{16,24},{18,... | collective-permute-start | bytes 1179656 | tf_op jit(solution)/shard_map/ppermute | solution.py:44
  154.9 50.0 %collective-permute-start.39 = (bf16[1024,128]{1,0:T(8,128)(2,1)S(1)}, bf16[1024,128]{1,0:T(8,128)(2,1)S(1)}, u32[]{:S(2)}, u32[]{:S(2)}) collective-permute-start(bf16[1024,128]{1,0:T(8,128)(2,1)S(1)} %copy-done.26), channel_id=1, source_target_pairs={{0,8},{2,10},{4,12},{6,14},{8,0},{10,2},{12,4},{14,6},{16,24},{18,... | collective-permute-start | bytes 786440 | tf_op jit(solution)/shard_map/ppermute | solution.py:44
  178.5 27.1 %collective-permute-start.47 = (bf16[1024,256]{1,0:T(8,128)(2,1)S(1)}, bf16[1024,256]{1,0:T(8,128)(2,1)S(1)}, u32[]{:S(2)}, u32[]{:S(2)}) collective-permute-start(bf16[1024,256]{1,0:T(8,128)(2,1)S(1)} %choose.11.refs_17_), channel_id=1, source_target_pairs={{0,2},{2,0},{4,6},{6,4},{8,10},{10,8},{12,14},{14,12},{16,18},{18,... | collective-permute-start | bytes 1572872 | tf_op jit(solution)/shard_map/ppermute | solution.py:44
  178.5 27.1 %collective-permute-start.41 = (bf16[1024,256]{1,0:T(8,128)(2,1)}, bf16[1024,256]{1,0:T(8,128)(2,1)S(1)}, u32[]{:S(2)}, u32[]{:S(2)}) collective-permute-start(bf16[1024,256]{1,0:T(8,128)(2,1)} %collective-permute-done.40.refs_15_), channel_id=1, source_target_pairs={{0,4},{2,6},{4,0},{6,2},{8,12},{10,14},{12,8},{14,10},{16,20},{18,... | collective-permute-start | bytes 1572872 | tf_op jit(solution)/shard_map/ppermute | solution.py:44
  179.2 26.5 %collective-permute-start.48 = (bf16[1024,256]{1,0:T(8,128)(2,1)S(1)}, bf16[1024,256]{1,0:T(8,128)(2,1)}, u32[]{:S(2)}, u32[]{:S(2)}) collective-permute-start(bf16[1024,256]{1,0:T(8,128)(2,1)S(1)} %collective-permute-done.46.refs_18_), channel_id=1, source_target_pairs={{0,2},{2,0},{4,6},{6,4},{8,10},{10,8},{12,14},{14,12},{16,18},{18,... | collective-permute-start | bytes 1572872 | tf_op jit(solution)/shard_map/ppermute | solution.py:44
  180.6 25.0 %collective-permute-start.36 = (bf16[256,256]{1,0:T(8,128)(2,1)S(1)}, bf16[256,256]{1,0:T(8,128)(2,1)S(1)}, u32[]{:S(2)}, u32[]{:S(2)}) collective-permute-start(bf16[256,256]{1,0:T(8,128)(2,1)S(1)} %get-tuple-element.40), channel_id=1, source_target_pairs={{0,16},{2,18},{4,20},{6,22},{8,24},{10,26},{12,28},{14,30},{16,0},... | collective-permute-start | bytes 393224 | tf_op jit(solution)/shard_map/ppermute | solution.py:44
  216.6 8.3 %collective-permute-start.49 = (bf16[512,2048]{1,0:T(8,128)(2,1)}, bf16[512,2048]{1,0:T(8,128)(2,1)S(1)}, u32[]{:S(2)}, u32[]{:S(2)}) collective-permute-start(bf16[512,2048]{1,0:T(8,128)(2,1)} %finish.3), channel_id=1, source_target_pairs={{0,1},{1,0},{2,3},{3,2},{4,5},{5,4},{6,7},{7,6},{8,9},{9,8},{10,11... | collective-permute-start | bytes 6291464 | tf_op jit(solution)/shard_map/ppermute | solution.py:44
  (39 other events, 544.1 us)
where the time goes:
time: 230 us; the launch traced here: 229 us
  waiting for transfers between devices  79.1 us (34%)
  Pallas kernels  71.6 us (31%)
  starting transfers between devices  52.8 us (23%)
  local copies, waits for them, and re-layouts  19.6 us (9%)
  other arithmetic  4.89 us (2%)
    ppermute x37, waiting for transfers between devices, flip(): return lax.ppermute(value, axis, pairs)  47.9 us
    ppermute x37, starting transfers between devices, flip(): return lax.ppermute(value, axis, pairs)  35.6 us
    ppermute x6, waiting for transfers between devices, hand_on(): return lax.ppermute(value, axis, pairs)  31.2 us
    pallas_call x2, Pallas kernels, finish(): pl.pallas_call(functools.partial(finish_body, channels=channels, parts=le...  16.2 us
    unnamed x80, local copies, waits for them, and re-layouts  16 us
    pallas_call x1, Pallas kernels, conv_project(): pl.pallas_call(functools.partial(conv_project_body, places=places), grid=...  12.6 us
    pallas_call x1, Pallas kernels, project(): pl.pallas_call(functools.partial(project_body, places=places), grid=(rows...  10.3 us
    pallas_call x1, Pallas kernels, convolve(): pl.pallas_call(conv_body, out_shape=[jax.ShapeDtypeStruct((rows, width),...  10 us
  transfers between devices with their start and end apart: 50, of which 16 were waited for; matrix products, arithmetic and copies ran while one was open for 4% of the time, Pallas kernels for 28%

commit v1 on v0

--- a/solution.py
+++ b/solution.py
@@ -545,20 +545,31 @@
     )(upper, packed, held)
 
 
+def enter_body(upper, packed, held, init, out):
+    last, logs = unpacking(packed)
+    above = upper[0] == 1
+    pre, pre_logs = held[:, :HV], held[:, HV : 2 * HV]
+    started = jnp.where(above, jnp.exp(pre_logs) * last + pre, pre)
+    logs = jnp.where(above, pre_logs + logs, pre_logs)
+    out[...] = (started + jnp.exp(logs) * init[...]).astype(bf16)
+
+
+def enter(held, packed, upper, init):
+    vmem = pl.BlockSpec(memory_space=pltpu.VMEM)
+    return pl.pallas_call(
+        enter_body,
+        in_specs=[SMEM, vmem, vmem, vmem],
+        out_specs=vmem,
+        out_shape=jax.ShapeDtypeStruct(init.shape, bf16),
+        compiler_params=pltpu.CompilerParams(vmem_limit_bytes=4 * 1024 * 1024),
+        name="enter",
+    )(upper, packed, held, init)
+
+
 def finish_body(start, offs, *refs, channels, parts, places):
     sums, refs = refs[:parts], refs[parts:]
-    conv, conv_gain, local, since, upper, packed, held, init, gate, head_gain, *refs = refs
-    weights, (out, state, act) = refs[: len(places)], refs[len(places) :]
-
-    @pl.when(pl.program_id(0) == 0)
-    def _():
-        last, logs = unpacking(packed)
-        above = upper[0] == 1
-        pre, pre_logs = held[:, :HV], held[:, HV : 2 * HV]
-        started = jnp.where(above, jnp.exp(pre_logs) * last + pre, pre)
-        logs = jnp.where(above, pre_logs + logs, pre_logs)
-        state[...] = (started + jnp.exp(logs) * init[...]).astype(bf16)
-
+    conv, conv_gain, local, since, state, gate, head_gain, *refs = refs
+    weights, (out, act) = refs[: len(places)], refs[len(places) :]
     width = conv.shape[1]
     stats = sums[0][...]
     for more in sums[1:]:
@@ -589,11 +600,10 @@
             out[:, there] = values[:, k * size : (k + 1) * size]
 
 
-def finish(first, rows, sums, conv, conv_gain, local, since, before, init, gate, head_gain, out_weights, total, channels):
+def finish(first, rows, sums, conv, conv_gain, local, since, state, gate, head_gain, out_weights, total, channels):
     pieces, places, offs = out_weights
     width, wide = conv.shape[1], local.shape[1]
     tile = min(ROW_TILE, rows)
-    held, packed, upper = before
     start = (first // tile).astype(jnp.int32).reshape(1)
 
     def tiled(cols):
@@ -612,16 +622,13 @@
             fixed((1, width)),
             tiled(wide),
             tiled(since.shape[1]),
-            SMEM,
-            fixed(packed.shape),
-            fixed(held.shape),
-            fixed(init.shape),
+            fixed(state.shape),
             tiled(wide),
             fixed((1, HV)),
         ]
         + [pl.BlockSpec(memory_space=pltpu.VMEM) for _ in pieces],
         out_specs=pl.BlockSpec((tile, total), lambda i, at: (i, 0)),
-        scratch_shapes=[pltpu.VMEM(init.shape, bf16), pltpu.VMEM((tile, width + wide), bf16)],
+        scratch_shapes=[pltpu.VMEM((tile, width + wide), bf16)],
     )
     return pl.pallas_call(
         functools.partial(finish_body, channels=channels, parts=len(sums), places=places),
@@ -632,7 +639,7 @@
             flops=2 * rows * (width + wide) * total, bytes_accessed=rows * total * 2, transcendentals=0
         ),
         name="finish",
-    )(start, offs, *sums, conv, conv_gain, local, since, upper, packed, held, init, gate, head_gain, *pieces)
+    )(start, offs, *sums, conv, conv_gain, local, since, state, gate, head_gain, *pieces)
 
 
 def normed_rows(own, axis, norm_gain):
@@ -693,7 +700,7 @@
     conv, sums = convolve(gated, gated_rim, conv_weight)
     sums = [sums, flip(sums, "tp", 1)] if groups == 2 else [lax.psum(sums, "tp")]
 
-    init = init_state.reshape(channels, HV)
+    state = enter(*before, init_state.reshape(channels, HV))
     total = norm_gain.shape[0]
 
     def rows_from(first, count):
@@ -705,8 +712,7 @@
             conv_gain[None, :],
             local,
             since,
-            before,
-            init,
+            state,
             gate,
             head_gain[None, :],
             out_weights,

time: 230 us -> 228 us (level)
    unnamed x80 -> x76, local copies, waits for them, and re-layouts: 16 us -> 15.1 us
where the time goes in v1:
time: 228 us; the launch traced here: 227 us
  waiting for transfers between devices  78.9 us (35%)
  Pallas kernels  70.9 us (31%)
  starting transfers between devices  52.9 us (23%)
  local copies, waits for them, and re-layouts  18.7 us (8%)
  other arithmetic  4.96 us (2%)
    ppermute x37, waiting for transfers between devices, flip(): return lax.ppermute(value, axis, pairs)  47.8 us
    ppermute x37, starting transfers between devices, flip(): return lax.ppermute(value, axis, pairs)  35.7 us
    ppermute x6, waiting for transfers between devices, hand_on(): return lax.ppermute(value, axis, pairs)  31.2 us
    pallas_call x2, Pallas kernels, finish(): pl.pallas_call(functools.partial(finish_body, channels=channels, parts=le...  15.4 us
    unnamed x76, local copies, waits for them, and re-layouts  15.1 us
    pallas_call x1, Pallas kernels, conv_project(): pl.pallas_call(functools.partial(conv_project_body, places=places), grid=...  12.6 us
    pallas_call x1, Pallas kernels, project(): pl.pallas_call(functools.partial(project_body, places=places), grid=(rows...  10.3 us
    pallas_call x1, Pallas kernels, convolve(): pl.pallas_call(conv_body, out_shape=[jax.ShapeDtypeStruct((rows, width),...  10 us
  transfers between devices with their start and end apart: 50, of which 16 were waited for; matrix products, arithmetic and copies ran while one was open for 4% of the time, Pallas kernels for 28%

profile of v1, /device:TPU:0, one launch (start us, length us, event | category | flops | bytes accessed | tf_op | source)
XLA Modules:
  0.0 227.1 jit_solution(8354218275210180343)
XLA Ops:
  3.9 2.6 %collective-permute-start.19 = (bf16[128,1280]{1,0:T(8,128)(2,1)S(1)}, bf16[128,1280]{1,0:T(8,128)(2,1)S(1)}, u32[]{:S(2)}, u32[]{:S(2)}) collective-permute-start(bf16[128,1280]{1,0:T(8,128)(2,1)S(1)} %constant_dynamic-update-slice_fusion.3.refs_0_), channel_id=1, source_target_pairs={{0,8},{2,10},{4,12},{6,14},{8,0},{10,2},{12,4},{14,6},{16,24},{18,... | collective-permute-start | bytes 983048 | tf_op jit(solution)/shard_map/ppermute | solution.py:44
  8.0 3.4 %collective-permute-start.1 = (bf16[32,1024]{1,0:T(8,128)(2,1)S(1)}, bf16[32,1024]{1,0:T(8,128)(2,1)S(1)}, u32[]{:S(2)}, u32[]{:S(2)}) collective-permute-start(bf16[32,1024]{1,0:T(8,128)(2,1)S(1)} %slice.3), channel_id=1, source_target_pairs={{0,2},{2,4},{4,6},{6,8},{8,10},{10,12},{12,14},{14,16},{16,18},{18... | collective-permute-start | bytes 196616 | tf_op jit(solution)/shard_map/ppermute | solution.py:168
  13.3 4.4 %collective-permute-start.37 = (bf16[1024,128]{1,0:T(8,128)(2,1)S(1)}, bf16[1024,128]{1,0:T(8,128)(2,1)S(1)}, u32[]{:S(2)}, u32[]{:S(2)}) collective-permute-start(bf16[1024,128]{1,0:T(8,128)(2,1)S(1)} %constant_dynamic-update-slice_fusion.7.refs_0_.refs_1_), channel_id=1, source_target_pairs={{0,8},{2,10},{4,12},{6,14},{8,0},{10,2},{12,4},{14,6},{16,24},{18,... | collective-permute-start | bytes 786440 | tf_op jit(solution)/shard_map/ppermute | solution.py:44
  20.0 1.5 collective-permute-start.17
  22.4 1.4 collective-permute-done.37.refs_2_.refs_3_
  23.9 1.7 collective-permute-start.3
  25.6 1.5 collective-permute-start.16
  27.8 2.2 collective-permute-done.17.refs_2_
  30.0 1.4 collective-permute-start.28
  31.3 2.5 %collective-permute-done.16.refs_1_ = bf16[128,1280]{1,0:T(8,128)(2,1)} collective-permute-done((bf16[128,1280]{1,0:T(8,128)(2,1)S(1)}, bf16[128,1280]{1,0:T(8,128)(2,1)}, u32[]{:S(2)}, u32[]{:S(2)}) %collective-permute-start.16) | collective-permute-done | bytes 327712 | tf_op jit(solution)/shard_map/ppermute | solution.py:44
  33.9 1.3 collective-permute-start.24
  35.2 1.6 collective-permute-start.20
  38.1 8.0 %collective-permute-done.24.refs_1_ = bf16[128,1280]{1,0:T(8,128)(2,1)S(1)} collective-permute-done((bf16[128,1280]{1,0:T(8,128)(2,1)S(1)}, bf16[128,1280]{1,0:T(8,128)(2,1)S(1)}, u32[]{:S(2)}, u32[]{:S(2)}) %collective-permute-start.24) | collective-permute-done | bytes 327712 | tf_op jit(solution)/shard_map/ppermute | solution.py:60
  46.8 1.3 collective-permute-start.29
  48.2 1.3 collective-permute-start.9
  49.6 1.3 collective-permute-start.11
  52.7 7.2 %collective-permute-done.29.refs_1_ = bf16[128,1280]{1,0:T(8,128)(2,1)} collective-permute-done((bf16[128,1280]{1,0:T(8,128)(2,1)}, bf16[128,1280]{1,0:T(8,128)(2,1)}, u32[]{:S(2)}, u32[]{:S(2)}) %collective-permute-start.29) | collective-permute-done | bytes 327712 | tf_op jit(solution)/shard_map/ppermute | solution.py:60
  60.2 1.9 choose.9.refs_12_
  63.1 5.2 %collective-permute-done.9.refs_1_ = bf16[128,1536]{1,0:T(8,128)(2,1)S(1)} collective-permute-done((bf16[128,1536]{1,0:T(8,128)(2,1)S(1)}, bf16[128,1536]{1,0:T(8,128)(2,1)S(1)}, u32[]{:S(2)}, u32[]{:S(2)}) %collective-permute-start.9) | collective-permute-done | bytes 393248 | tf_op jit(solution)/shard_map/ppermute | solution.py:60
  70.2 3.8 %collective-permute-done.11.refs_3_ = bf16[128,1536]{1,0:T(8,128)(2,1)S(1)} collective-permute-done((bf16[128,1536]{1,0:T(8,128)(2,1)S(1)}, bf16[128,1536]{1,0:T(8,128)(2,1)S(1)}, u32[]{:S(2)}, u32[]{:S(2)}) %collective-permute-start.11) | collective-permute-done | bytes 393248 | tf_op jit(solution)/shard_map/ppermute | solution.py:60
  75.8 1.5 collective-permute-start.32
  80.0 6.0 %normalize.2.normed = bf16[1024,2048]{1,0:T(8,128)(2,1)} custom-call(s32[2]{0:T(128)} %add_multiply_fusion.places, bf16[1024,1024]{1,0:T(8,128)(2,1)} %refs_0_.1, bf16[1024,1024]{1,0:T(8,128)(2,1)} %collective-permute-done.refs_1_, f32[1,2048]{1,0:T(1,128)} %bitcast.16), custom_call_target="tpu_custom_call" | custom-call | tf_op jit(solution)/shard_map/normalize/pallas_call | solution.py:235
  86.1 1.5 collective-permute-start.4
  87.5 1.4 collective-permute-start.42
  91.0 3.1 %collective-permute-done.32.refs_15_ = bf16[128,1280]{1,0:T(8,128)(2,1)} collective-permute-done((bf16[128,1280]{1,0:T(8,128)(2,1)}, bf16[128,1280]{1,0:T(8,128)(2,1)}, u32[]{:S(2)}, u32[]{:S(2)}) %collective-permute-start.32) | collective-permute-done | bytes 327712 | tf_op jit(solution)/shard_map/ppermute | solution.py:44
  94.1 1.6 collective-permute-start.12
  95.7 10.3 %project.1 = (bf16[1024,256]{1,0:T(8,128)(2,1)}, bf16[1024,256]{1,0:T(8,128)(2,1)}, bf16[1024,512]{1,0:T(8,128)(2,1)}, f32[1024,256]{1,0:T(8,128)}) custom-call(s32[24]{0:T(128)} %fusion.offs, bf16[1024,2048]{1,0:T(8,128)(2,1)} %normalize.2.normed, bf16[128,1280]{1,0:T(8,128)(2,1)} %copy-done.28, bf16[128,1280]{1,0:T(8,128)(2,1)} %collective-permute-done.16.refs_1_, ...), custom_call_target="tpu_custom_call" | custom-call | flops 5368709120 | bytes 4194304 | tf_op jit(solution)/shard_map/project/pallas_call | solution.py:279
  110.5 9.2 %linear_attention.1 = (bf16[1024,512]{1,0:T(8,128)(2,1)S(1)}, bf16[1024,256]{1,0:T(8,128)(2,1)S(1)}, f32[256,512]{1,0:T(8,128)S(1)}, bf16[256,256]{1,0:T(8,128)(2,1)S(1)}) custom-call(bf16[1024,256]{1,0:T(8,128)(2,1)S(1)} %copy-done.20, bf16[1024,256]{1,0:T(8,128)(2,1)S(1)} %copy-done.21, bf16[1024,512]{1,0:T(8,128)(2,1)S(1)} %copy-done.18, ...), custom_call_target="tpu_custom_call" | custom-call | flops 1342177280 | bytes 4194304 | tf_op jit(solution)/shard_map/linear_attention/pallas_call | solution.py:484
  120.2 1.4 collective-permute-start.44
  121.6 1.3 collective-permute-start.43
  123.0 3.2 %collective-permute-done.33.packed = bf16[256,256]{1,0:T(8,128)(2,1)S(1)} collective-permute-done((bf16[256,256]{1,0:T(8,128)(2,1)S(1)}, bf16[256,256]{1,0:T(8,128)(2,1)S(1)}, u32[]{:S(2)}, u32[]{:S(2)}) %collective-permute-start.33) | collective-permute-done | bytes 131104 | tf_op jit(solution)/shard_map/ppermute | solution.py:44
  126.9 4.8 %collective-permute-done.43.refs_1_ = bf16[1024,128]{1,0:T(8,128)(2,1)} collective-permute-done((bf16[1024,128]{1,0:T(8,128)(2,1)}, bf16[1024,128]{1,0:T(8,128)(2,1)}, u32[]{:S(2)}, u32[]{:S(2)}) %collective-permute-start.43) | collective-permute-done | bytes 262176 | tf_op jit(solution)/shard_map/ppermute | solution.py:60
  131.7 1.3 collective-permute-start.45
  133.1 2.9 %collective-permute-start.7 = (bf16[256,1536]{1,0:T(8,128)(2,1)}, bf16[256,1536]{1,0:T(8,128)(2,1)}, u32[]{:S(2)}, u32[]{:S(2)}) collective-permute-start(bf16[256,1536]{1,0:T(8,128)(2,1)} %collective-permute-done.6.refs_3_), channel_id=1, source_target_pairs={{0,2},{2,0},{4,6},{6,4},{8,10},{10,8},{12,14},{14,12},{16,18},{18,... | collective-permute-start | bytes 2359304 | tf_op jit(solution)/shard_map/ppermute | solution.py:44
  136.0 1.9 collective-permute-start.14
  138.1 2.1 collective-permute-done.45.refs_3_
  140.9 1.4 choose.11.refs_14_
  142.4 3.4 %collective-permute-done.35.packed = bf16[256,256]{1,0:T(8,128)(2,1)S(1)} collective-permute-done((bf16[256,256]{1,0:T(8,128)(2,1)S(1)}, bf16[256,256]{1,0:T(8,128)(2,1)S(1)}, u32[]{:S(2)}, u32[]{:S(2)}) %collective-permute-start.35) | collective-permute-done | bytes 131104 | tf_op jit(solution)/shard_map/ppermute | solution.py:44
  146.0 1.7 normalize.3.before
  147.9 7.3 %collective-permute-done.5.refs_2_ = bf16[128,1536]{1,0:T(8,128)(2,1)} collective-permute-done((bf16[128,1536]{1,0:T(8,128)(2,1)}, bf16[128,1536]{1,0:T(8,128)(2,1)}, u32[]{:S(2)}, u32[]{:S(2)}) %collective-permute-start.5) | collective-permute-done | bytes 393248 | tf_op jit(solution)/shard_map/ppermute | solution.py:44
  155.4 23.1 %collective-permute-done.46.refs_15_ = bf16[1024,256]{1,0:T(8,128)(2,1)S(1)} collective-permute-done((bf16[1024,256]{1,0:T(8,128)(2,1)S(1)}, bf16[1024,256]{1,0:T(8,128)(2,1)S(1)}, u32[]{:S(2)}, u32[]{:S(2)}) %collective-permute-start.46) | collective-permute-done | bytes 524320 | tf_op jit(solution)/shard_map/ppermute | solution.py:44
  179.2 1.4 collective-permute-start.48
  180.6 1.6 collective-permute-start.36
  182.2 12.6 %conv_project.1 = (bf16[1024,512]{1,0:T(8,128)(2,1)}, bf16[1024,512]{1,0:T(8,128)(2,1)}, bf16[32,512]{1,0:T(8,128)(2,1)}) custom-call(s32[24]{0:T(128)} %fusion.offs, bf16[1024,2048]{1,0:T(8,128)(2,1)} %normalize.2.normed, bf16[32,2048]{1,0:T(8,128)(2,1)} %normalize.3.before, bf16[256,1536]{1,0:T(8,128)(2,1)} %copy-done.4, ...), custom_call_target="tpu_custom_call" | custom-call | flops 6442450944 | bytes 4194304 | tf_op jit(solution)/shard_map/conv_project/pallas_call | solution.py:318
  194.8 10.0 %convolve.1 = (bf16[1024,512]{1,0:T(8,128)(2,1)}, f32[1024,2]{1,0:T(8,128)}) custom-call(bf16[1024,512]{1,0:T(8,128)(2,1)} %get-tuple-element.24.gated, bf16[32,512]{1,0:T(8,128)(2,1)} %get-tuple-element.25.rim, f32[31,512]{1,0:T(8,128)} %taps.1), custom_call_target="tpu_custom_call" | custom-call | flops 325058560 | bytes 3145728 | tf_op jit(solution)/shard_map/convolve/pallas_call | solution.py:383
  207.8 7.7 %finish.3 = bf16[512,2048]{1,0:T(8,128)(2,1)} custom-call(s32[1]{0:T(128)} %bitcast.13.start, s32[24]{0:T(128)} %fusion.offs, f32[1024,2]{1,0:T(8,128)} %get-tuple-element.26.refs_0_, f32[1024,2]{1,0:T(8,128)} %copy-done.24, bf16[1024,512]{1,0:T(8,128)(2,1)} %get-tuple-element.27.refs_2_, f32[1,512]{1,0:T(1,128)} %bitcast.18, bf16[1024,512]{1,0:T(8,128)(2,1)} %copy-done.2, ...), custom_call_target="tpu_custom_call" | custom-call | flops 2147483648 | bytes 2097152 | tf_op jit(solution)/shard_map/finish/pallas_call | solution.py:633
  215.6 7.7 %finish.2 = bf16[512,2048]{1,0:T(8,128)(2,1)} custom-call(s32[1]{0:T(128)} %bitcast.start, s32[24]{0:T(128)} %fusion.offs, f32[1024,2]{1,0:T(8,128)} %get-tuple-element.26.refs_0_, f32[1024,2]{1,0:T(8,128)} %copy-done.24, bf16[1024,512]{1,0:T(8,128)(2,1)} %get-tuple-element.27.refs_2_, f32[1,512]{1,0:T(1,128)} %bitcast.19, bf16[1024,512]{1,0:T(8,128)(2,1)} %copy-done.2, ...), custom_call_target="tpu_custom_call" | custom-call | flops 2147483648 | bytes 2097152 | tf_op jit(solution)/shard_map/finish/pallas_call | solution.py:633
  223.4 3.7 %add_convert_fusion = bf16[512,2048]{1,0:T(8,128)(2,1)} fusion(bf16[512,2048]{1,0:T(8,128)(2,1)S(1)} %collective-permute-done.49, bf16[512,2048]{1,0:T(8,128)(2,1)} %finish.2), kind=kLoop, calls=%fused_computation | loop fusion | flops 4194304 | bytes 6291456 | tf_op jit(solution)/shard_map/convert_element_type | solution.py:729
  (155 shorter events, 36.1 us)
Async XLA Ops:
  0.0 75.8 %collective-permute-start = (bf16[1024,1024]{1,0:T(8,128)(2,1)}, bf16[1024,1024]{1,0:T(8,128)(2,1)}, u32[]{:S(2)}, u32[]{:S(2)}) collective-permute-start(bf16[1024,1024]{1,0:T(8,128)(2,1)} %refs_0_.1), channel_id=1, source_target_pairs={{0,1},{1,0},{2,3},{3,2},{4,5},{5,4},{6,7},{7,6},{8,9},{9,8},{10,11... | collective-permute-start | bytes 6291464 | tf_op jit(solution)/shard_map/ppermute | solution.py:44
  3.9 21.7 %collective-permute-start.19 = (bf16[128,1280]{1,0:T(8,128)(2,1)S(1)}, bf16[128,1280]{1,0:T(8,128)(2,1)S(1)}, u32[]{:S(2)}, u32[]{:S(2)}) collective-permute-start(bf16[128,1280]{1,0:T(8,128)(2,1)S(1)} %constant_dynamic-update-slice_fusion.3.refs_0_), channel_id=1, source_target_pairs={{0,8},{2,10},{4,12},{6,14},{8,0},{10,2},{12,4},{14,6},{16,24},{18,... | collective-permute-start | bytes 983048 | tf_op jit(solution)/shard_map/ppermute | solution.py:44
  6.5 20.6 %collective-permute-start.23 = (bf16[128,1280]{1,0:T(8,128)(2,1)S(1)}, bf16[128,1280]{1,0:T(8,128)(2,1)S(1)}, u32[]{:S(2)}, u32[]{:S(2)}) collective-permute-start(bf16[128,1280]{1,0:T(8,128)(2,1)S(1)} %constant_dynamic-update-slice_fusion.3.refs_0_), channel_id=1, source_target_pairs={{8,16},{10,18},{12,20},{14,22},{16,8},{18,10},{20,12},{22,14},{9,1... | collective-permute-start | bytes 983048 | tf_op jit(solution)/shard_map/ppermute | solution.py:54
  8.0 10.6 %collective-permute-start.1 = (bf16[32,1024]{1,0:T(8,128)(2,1)S(1)}, bf16[32,1024]{1,0:T(8,128)(2,1)S(1)}, u32[]{:S(2)}, u32[]{:S(2)}) collective-permute-start(bf16[32,1024]{1,0:T(8,128)(2,1)S(1)} %slice.3), channel_id=1, source_target_pairs={{0,2},{2,4},{4,6},{6,8},{8,10},{10,12},{12,14},{14,16},{16,18},{18... | collective-permute-start | bytes 196616 | tf_op jit(solution)/shard_map/ppermute | solution.py:168
  13.3 10.6 %collective-permute-start.37 = (bf16[1024,128]{1,0:T(8,128)(2,1)S(1)}, bf16[1024,128]{1,0:T(8,128)(2,1)S(1)}, u32[]{:S(2)}, u32[]{:S(2)}) collective-permute-start(bf16[1024,128]{1,0:T(8,128)(2,1)S(1)} %constant_dynamic-update-slice_fusion.7.refs_0_.refs_1_), channel_id=1, source_target_pairs={{0,8},{2,10},{4,12},{6,14},{8,0},{10,2},{12,4},{14,6},{16,24},{18,... | collective-permute-start | bytes 786440 | tf_op jit(solution)/shard_map/ppermute | solution.py:44
  20.0 10.0 %collective-permute-start.17 = (bf16[128,1280]{1,0:T(8,128)(2,1)S(1)}, bf16[128,1280]{1,0:T(8,128)(2,1)}, u32[]{:S(2)}, u32[]{:S(2)}) collective-permute-start(bf16[128,1280]{1,0:T(8,128)(2,1)S(1)} %constant_dynamic-update-slice_fusion.3.refs_0_), channel_id=1, source_target_pairs={{0,4},{2,6},{4,0},{6,2},{8,12},{10,14},{12,8},{14,10},{16,20},{18,... | collective-permute-start | bytes 983048 | tf_op jit(solution)/shard_map/ppermute | solution.py:44
  23.9 11.3 %collective-permute-start.3 = (bf16[128,1536]{1,0:T(8,128)(2,1)S(1)}, bf16[128,1536]{1,0:T(8,128)(2,1)S(1)}, u32[]{:S(2)}, u32[]{:S(2)}) collective-permute-start(bf16[128,1536]{1,0:T(8,128)(2,1)S(1)} %constant_dynamic-update-slice_fusion.refs_0_.refs_1_), channel_id=1, source_target_pairs={{0,8},{2,10},{4,12},{6,14},{8,0},{10,2},{12,4},{14,6},{16,24},{18,... | collective-permute-start | bytes 1179656 | tf_op jit(solution)/shard_map/ppermute | solution.py:44
  25.6 8.3 %collective-permute-start.16 = (bf16[128,1280]{1,0:T(8,128)(2,1)S(1)}, bf16[128,1280]{1,0:T(8,128)(2,1)}, u32[]{:S(2)}, u32[]{:S(2)}) collective-permute-start(bf16[128,1280]{1,0:T(8,128)(2,1)S(1)} %constant_dynamic-update-slice_fusion.3.refs_0_), channel_id=1, source_target_pairs={{0,2},{2,0},{4,6},{6,4},{8,10},{10,8},{12,14},{14,12},{16,18},{18,... | collective-permute-start | bytes 983048 | tf_op jit(solution)/shard_map/ppermute | solution.py:44
  27.1 9.6 %collective-permute-start.8 = (bf16[128,1536]{1,0:T(8,128)(2,1)S(1)}, bf16[128,1536]{1,0:T(8,128)(2,1)S(1)}, u32[]{:S(2)}, u32[]{:S(2)}) collective-permute-start(bf16[128,1536]{1,0:T(8,128)(2,1)S(1)} %constant_dynamic-update-slice_fusion.refs_0_.refs_1_), channel_id=1, source_target_pairs={{8,16},{10,18},{12,20},{14,22},{16,8},{18,10},{20,12},{22,14},{9,1... | collective-permute-start | bytes 1179656 | tf_op jit(solution)/shard_map/ppermute | solution.py:54
  30.0 7.4 %collective-permute-start.28 = (bf16[128,1280]{1,0:T(8,128)(2,1)S(1)}, bf16[128,1280]{1,0:T(8,128)(2,1)}, u32[]{:S(2)}, u32[]{:S(2)}) collective-permute-start(bf16[128,1280]{1,0:T(8,128)(2,1)S(1)} %collective-permute-done.19.refs_4_), channel_id=1, source_target_pairs={{8,16},{10,18},{12,20},{14,22},{16,8},{18,10},{20,12},{22,14},{9,1... | collective-permute-start | bytes 983048 | tf_op jit(solution)/shard_map/ppermute | solution.py:54
  33.9 12.2 %collective-permute-start.24 = (bf16[128,1280]{1,0:T(8,128)(2,1)S(1)}, bf16[128,1280]{1,0:T(8,128)(2,1)S(1)}, u32[]{:S(2)}, u32[]{:S(2)}) collective-permute-start(bf16[128,1280]{1,0:T(8,128)(2,1)S(1)} %collective-permute-done.23.refs_0_), channel_id=1, source_target_pairs={{8,0},{10,2},{12,4},{14,6},{16,24},{18,26},{20,28},{22,30},{9,1},{... | collective-permute-start | bytes 983048 | tf_op jit(solution)/shard_map/ppermute | solution.py:60
  35.2 13.0 %collective-permute-start.20 = (bf16[128,1280]{1,0:T(8,128)(2,1)S(1)}, bf16[128,1280]{1,0:T(8,128)(2,1)}, u32[]{:S(2)}, u32[]{:S(2)}) collective-permute-start(bf16[128,1280]{1,0:T(8,128)(2,1)S(1)} %collective-permute-done.19.refs_4_), channel_id=1, source_target_pairs={{0,2},{2,0},{4,6},{6,4},{8,10},{10,8},{12,14},{14,12},{16,18},{18,... | collective-permute-start | bytes 983048 | tf_op jit(solution)/shard_map/ppermute | solution.py:44
  36.7 12.8 %collective-permute-start.10 = (bf16[128,1536]{1,0:T(8,128)(2,1)S(1)}, bf16[128,1536]{1,0:T(8,128)(2,1)S(1)}, u32[]{:S(2)}, u32[]{:S(2)}) collective-permute-start(bf16[128,1536]{1,0:T(8,128)(2,1)S(1)} %collective-permute-done.3.refs_2_.refs_3_), channel_id=1, source_target_pairs={{8,16},{10,18},{12,20},{14,22},{16,8},{18,10},{20,12},{22,14},{9,1... | collective-permute-start | bytes 1179656 | tf_op jit(solution)/shard_map/ppermute | solution.py:54
  37.4 10.8 %collective-permute-start.21 = (bf16[128,1280]{1,0:T(8,128)(2,1)S(1)}, bf16[128,1280]{1,0:T(8,128)(2,1)S(1)}, u32[]{:S(2)}, u32[]{:S(2)}) collective-permute-start(bf16[128,1280]{1,0:T(8,128)(2,1)S(1)} %collective-permute-done.19.refs_4_), channel_id=1, source_target_pairs={{0,4},{2,6},{4,0},{6,2},{8,12},{10,14},{12,8},{14,10},{16,20},{18,... | collective-permute-start | bytes 983048 | tf_op jit(solution)/shard_map/ppermute | solution.py:44
  46.8 13.1 %collective-permute-start.29 = (bf16[128,1280]{1,0:T(8,128)(2,1)}, bf16[128,1280]{1,0:T(8,128)(2,1)}, u32[]{:S(2)}, u32[]{:S(2)}) collective-permute-start(bf16[128,1280]{1,0:T(8,128)(2,1)} %collective-permute-done.28.refs_0_), channel_id=1, source_target_pairs={{8,0},{10,2},{12,4},{14,6},{16,24},{18,26},{20,28},{22,30},{9,1},{... | collective-permute-start | bytes 983048 | tf_op jit(solution)/shard_map/ppermute | solution.py:60
  48.1 14.0 %collective-permute-start.18 = (bf16[128,1280]{1,0:T(8,128)(2,1)}, bf16[128,1280]{1,0:T(8,128)(2,1)}, u32[]{:S(2)}, u32[]{:S(2)}) collective-permute-start(bf16[128,1280]{1,0:T(8,128)(2,1)} %collective-permute-done.17.refs_2_), channel_id=1, source_target_pairs={{0,2},{2,0},{4,6},{6,4},{8,10},{10,8},{12,14},{14,12},{16,18},{18,... | collective-permute-start | bytes 983048 | tf_op jit(solution)/shard_map/ppermute | solution.py:44
  48.2 20.0 %collective-permute-start.9 = (bf16[128,1536]{1,0:T(8,128)(2,1)S(1)}, bf16[128,1536]{1,0:T(8,128)(2,1)S(1)}, u32[]{:S(2)}, u32[]{:S(2)}) collective-permute-start(bf16[128,1536]{1,0:T(8,128)(2,1)S(1)} %collective-permute-done.8.refs_0_), channel_id=1, source_target_pairs={{8,0},{10,2},{12,4},{14,6},{16,24},{18,26},{20,28},{22,30},{9,1},{... | collective-permute-start | bytes 1179656 | tf_op jit(solution)/shard_map/ppermute | solution.py:60
  49.6 24.4 %collective-permute-start.11 = (bf16[128,1536]{1,0:T(8,128)(2,1)S(1)}, bf16[128,1536]{1,0:T(8,128)(2,1)S(1)}, u32[]{:S(2)}, u32[]{:S(2)}) collective-permute-start(bf16[128,1536]{1,0:T(8,128)(2,1)S(1)} %collective-permute-done.10.refs_2_), channel_id=1, source_target_pairs={{8,0},{10,2},{12,4},{14,6},{16,24},{18,26},{20,28},{22,30},{9,1},{... | collective-permute-start | bytes 1179656 | tf_op jit(solution)/shard_map/ppermute | solution.py:60
  59.9 10.2 %collective-permute-start.26 = (bf16[128,1280]{1,0:T(8,128)(2,1)}, bf16[128,1280]{1,0:T(8,128)(2,1)}, u32[]{:S(2)}, u32[]{:S(2)}) collective-permute-start(bf16[128,1280]{1,0:T(8,128)(2,1)} %choose.8.refs_8_), channel_id=1, source_target_pairs={{0,4},{2,6},{4,0},{6,2},{8,12},{10,14},{12,8},{14,10},{16,20},{18,... | collective-permute-start | bytes 983048 | tf_op jit(solution)/shard_map/ppermute | solution.py:44
  62.1 13.5 %collective-permute-start.30 = (bf16[128,1280]{1,0:T(8,128)(2,1)}, bf16[128,1280]{1,0:T(8,128)(2,1)}, u32[]{:S(2)}, u32[]{:S(2)}) collective-permute-start(bf16[128,1280]{1,0:T(8,128)(2,1)} %choose.9.refs_12_), channel_id=1, source_target_pairs={{0,2},{2,0},{4,6},{6,4},{8,10},{10,8},{12,14},{14,12},{16,18},{18,... | collective-permute-start | bytes 983048 | tf_op jit(solution)/shard_map/ppermute | solution.py:44
  69.0 17.1 %collective-permute-start.25 = (bf16[128,1280]{1,0:T(8,128)(2,1)}, bf16[128,1280]{1,0:T(8,128)(2,1)S(1)}, u32[]{:S(2)}, u32[]{:S(2)}) collective-permute-start(bf16[128,1280]{1,0:T(8,128)(2,1)} %choose.8.refs_8_), channel_id=1, source_target_pairs={{0,2},{2,0},{4,6},{6,4},{8,10},{10,8},{12,14},{14,12},{16,18},{18,... | collective-permute-start | bytes 983048 | tf_op jit(solution)/shard_map/ppermute | solution.py:44
  70.2 17.4 %collective-permute-start.22 = (bf16[128,1280]{1,0:T(8,128)(2,1)}, bf16[128,1280]{1,0:T(8,128)(2,1)S(1)}, u32[]{:S(2)}, u32[]{:S(2)}) collective-permute-start(bf16[128,1280]{1,0:T(8,128)(2,1)} %collective-permute-done.20.refs_5_), channel_id=1, source_target_pairs={{0,4},{2,6},{4,0},{6,2},{8,12},{10,14},{12,8},{14,10},{16,20},{18,... | collective-permute-start | bytes 983048 | tf_op jit(solution)/shard_map/ppermute | solution.py:44
  74.7 14.2 %collective-permute-start.31 = (bf16[128,1280]{1,0:T(8,128)(2,1)}, bf16[128,1280]{1,0:T(8,128)(2,1)S(1)}, u32[]{:S(2)}, u32[]{:S(2)}) collective-permute-start(bf16[128,1280]{1,0:T(8,128)(2,1)} %choose.9.refs_12_), channel_id=1, source_target_pairs={{0,4},{2,6},{4,0},{6,2},{8,12},{10,14},{12,8},{14,10},{16,20},{18,... | collective-permute-start | bytes 983048 | tf_op jit(solution)/shard_map/ppermute | solution.py:44
  75.6 14.2 %collective-permute-start.27 = (bf16[128,1280]{1,0:T(8,128)(2,1)}, bf16[128,1280]{1,0:T(8,128)(2,1)S(1)}, u32[]{:S(2)}, u32[]{:S(2)}) collective-permute-start(bf16[128,1280]{1,0:T(8,128)(2,1)} %collective-permute-done.26.refs_10_), channel_id=1, source_target_pairs={{0,2},{2,0},{4,6},{6,4},{8,10},{10,8},{12,14},{14,12},{16,18},{18,... | collective-permute-start | bytes 983048 | tf_op jit(solution)/shard_map/ppermute | solution.py:44
  75.8 18.2 %collective-permute-start.32 = (bf16[128,1280]{1,0:T(8,128)(2,1)}, bf16[128,1280]{1,0:T(8,128)(2,1)}, u32[]{:S(2)}, u32[]{:S(2)}) collective-permute-start(bf16[128,1280]{1,0:T(8,128)(2,1)} %collective-permute-done.30.refs_13_), channel_id=1, source_target_pairs={{0,4},{2,6},{4,0},{6,2},{8,12},{10,14},{12,8},{14,10},{16,20},{18,... | collective-permute-start | bytes 983048 | tf_op jit(solution)/shard_map/ppermute | solution.py:44
  86.1 35.5 %collective-permute-start.4 = (bf16[128,1536]{1,0:T(8,128)(2,1)S(1)}, bf16[128,1536]{1,0:T(8,128)(2,1)}, u32[]{:S(2)}, u32[]{:S(2)}) collective-permute-start(bf16[128,1536]{1,0:T(8,128)(2,1)S(1)} %constant_dynamic-update-slice_fusion.refs_0_.refs_1_), channel_id=1, source_target_pairs={{0,2},{2,0},{4,6},{6,4},{8,10},{10,8},{12,14},{14,12},{16,18},{18,... | collective-permute-start | bytes 1179656 | tf_op jit(solution)/shard_map/ppermute | solution.py:44
  87.5 32.2 %collective-permute-start.42 = (bf16[1024,128]{1,0:T(8,128)(2,1)S(1)}, bf16[1024,128]{1,0:T(8,128)(2,1)}, u32[]{:S(2)}, u32[]{:S(2)}) collective-permute-start(bf16[1024,128]{1,0:T(8,128)(2,1)S(1)} %constant_dynamic-update-slice_fusion.7.refs_0_.refs_1_), channel_id=1, source_target_pairs={{8,16},{10,18},{12,20},{14,22},{16,8},{18,10},{20,12},{22,14},{9,1... | collective-permute-start | bytes 786440 | tf_op jit(solution)/shard_map/ppermute | solution.py:54
  88.9 31.3 %collective-permute-start.38 = (bf16[1024,128]{1,0:T(8,128)(2,1)S(1)}, bf16[1024,128]{1,0:T(8,128)(2,1)}, u32[]{:S(2)}, u32[]{:S(2)}) collective-permute-start(bf16[1024,128]{1,0:T(8,128)(2,1)S(1)} %constant_dynamic-update-slice_fusion.7.refs_0_.refs_1_), channel_id=1, source_target_pairs={{0,4},{2,6},{4,0},{6,2},{8,12},{10,14},{12,8},{14,10},{16,20},{18,... | collective-permute-start | bytes 786440 | tf_op jit(solution)/shard_map/ppermute | solution.py:44
  89.8 43.3 %collective-permute-start.6 = (bf16[256,1536]{1,0:T(8,128)(2,1)S(1)}, bf16[256,1536]{1,0:T(8,128)(2,1)}, u32[]{:S(2)}, u32[]{:S(2)}) collective-permute-start(bf16[256,1536]{1,0:T(8,128)(2,1)S(1)} %choose.6.refs_0_), channel_id=1, source_target_pairs={{0,4},{2,6},{4,0},{6,2},{8,12},{10,14},{12,8},{14,10},{16,20},{18,... | collective-permute-start | bytes 2359304 | tf_op jit(solution)/shard_map/ppermute | solution.py:44
  94.1 39.0 %collective-permute-start.12 = (bf16[256,1536]{1,0:T(8,128)(2,1)S(1)}, bf16[256,1536]{1,0:T(8,128)(2,1)}, u32[]{:S(2)}, u32[]{:S(2)}) collective-permute-start(bf16[256,1536]{1,0:T(8,128)(2,1)S(1)} %choose.7.refs_5_), channel_id=1, source_target_pairs={{0,2},{2,0},{4,6},{6,4},{8,10},{10,8},{12,14},{14,12},{16,18},{18,... | collective-permute-start | bytes 2359304 | tf_op jit(solution)/shard_map/ppermute | solution.py:44
  119.7 6.4 %collective-permute-start.33 = (bf16[256,256]{1,0:T(8,128)(2,1)S(1)}, bf16[256,256]{1,0:T(8,128)(2,1)S(1)}, u32[]{:S(2)}, u32[]{:S(2)}) collective-permute-start(bf16[256,256]{1,0:T(8,128)(2,1)S(1)} %get-tuple-element.34), channel_id=1, source_target_pairs={{0,2},{2,0},{4,6},{6,4},{8,10},{10,8},{12,14},{14,12},{16,18},{18,... | collective-permute-start | bytes 393224 | tf_op jit(solution)/shard_map/ppermute | solution.py:44
  120.2 6.6 %collective-permute-start.44 = (bf16[1024,128]{1,0:T(8,128)(2,1)S(1)}, bf16[1024,128]{1,0:T(8,128)(2,1)}, u32[]{:S(2)}, u32[]{:S(2)}) collective-permute-start(bf16[1024,128]{1,0:T(8,128)(2,1)S(1)} %collective-permute-done.37.refs_2_.refs_3_), channel_id=1, source_target_pairs={{8,16},{10,18},{12,20},{14,22},{16,8},{18,10},{20,12},{22,14},{9,1... | collective-permute-start | bytes 786440 | tf_op jit(solution)/shard_map/ppermute | solution.py:54
  121.6 10.1 %collective-permute-start.43 = (bf16[1024,128]{1,0:T(8,128)(2,1)}, bf16[1024,128]{1,0:T(8,128)(2,1)}, u32[]{:S(2)}, u32[]{:S(2)}) collective-permute-start(bf16[1024,128]{1,0:T(8,128)(2,1)} %collective-permute-done.42.refs_0_), channel_id=1, source_target_pairs={{8,0},{10,2},{12,4},{14,6},{16,24},{18,26},{20,28},{22,30},{9,1},{... | collective-permute-start | bytes 786440 | tf_op jit(solution)/shard_map/ppermute | solution.py:60
  126.2 16.1 %collective-permute-start.40 = (bf16[1024,256]{1,0:T(8,128)(2,1)S(1)}, bf16[1024,256]{1,0:T(8,128)(2,1)}, u32[]{:S(2)}, u32[]{:S(2)}) collective-permute-start(bf16[1024,256]{1,0:T(8,128)(2,1)S(1)} %choose.10.refs_9_), channel_id=1, source_target_pairs={{0,2},{2,0},{4,6},{6,4},{8,10},{10,8},{12,14},{14,12},{16,18},{18,... | collective-permute-start | bytes 1572872 | tf_op jit(solution)/shard_map/ppermute | solution.py:44
  126.8 9.2 %collective-permute-start.34 = (bf16[256,256]{1,0:T(8,128)(2,1)S(1)}, bf16[256,256]{1,0:T(8,128)(2,1)S(1)}, u32[]{:S(2)}, u32[]{:S(2)}) collective-permute-start(bf16[256,256]{1,0:T(8,128)(2,1)S(1)} %get-tuple-element.36), channel_id=1, source_target_pairs={{0,4},{2,6},{4,0},{6,2},{8,12},{10,14},{12,8},{14,10},{16,20},{18,... | collective-permute-start | bytes 393224 | tf_op jit(solution)/shard_map/ppermute | solution.py:44
  131.7 8.5 %collective-permute-start.45 = (bf16[1024,128]{1,0:T(8,128)(2,1)}, bf16[1024,128]{1,0:T(8,128)(2,1)S(1)}, u32[]{:S(2)}, u32[]{:S(2)}) collective-permute-start(bf16[1024,128]{1,0:T(8,128)(2,1)} %collective-permute-done.44.refs_2_), channel_id=1, source_target_pairs={{8,0},{10,2},{12,4},{14,6},{16,24},{18,26},{20,28},{22,30},{9,1},{... | collective-permute-start | bytes 786440 | tf_op jit(solution)/shard_map/ppermute | solution.py:60
  133.0 45.5 %collective-permute-start.13 = (bf16[256,1536]{1,0:T(8,128)(2,1)S(1)}, bf16[256,1536]{1,0:T(8,128)(2,1)}, u32[]{:S(2)}, u32[]{:S(2)}) collective-permute-start(bf16[256,1536]{1,0:T(8,128)(2,1)S(1)} %choose.7.refs_5_), channel_id=1, source_target_pairs={{0,4},{2,6},{4,0},{6,2},{8,12},{10,14},{12,8},{14,10},{16,20},{18,... | collective-permute-start | bytes 2359304 | tf_op jit(solution)/shard_map/ppermute | solution.py:44
  133.1 46.0 %collective-permute-start.7 = (bf16[256,1536]{1,0:T(8,128)(2,1)}, bf16[256,1536]{1,0:T(8,128)(2,1)}, u32[]{:S(2)}, u32[]{:S(2)}) collective-permute-start(bf16[256,1536]{1,0:T(8,128)(2,1)} %collective-permute-done.6.refs_3_), channel_id=1, source_target_pairs={{0,2},{2,0},{4,6},{6,4},{8,10},{10,8},{12,14},{14,12},{16,18},{18,... | collective-permute-start | bytes 2359304 | tf_op jit(solution)/shard_map/ppermute | solution.py:44
  136.0 44.6 %collective-permute-start.14 = (bf16[256,1536]{1,0:T(8,128)(2,1)}, bf16[256,1536]{1,0:T(8,128)(2,1)}, u32[]{:S(2)}, u32[]{:S(2)}) collective-permute-start(bf16[256,1536]{1,0:T(8,128)(2,1)} %collective-permute-done.12.refs_6_), channel_id=1, source_target_pairs={{0,4},{2,6},{4,0},{6,2},{8,12},{10,14},{12,8},{14,10},{16,20},{18,... | collective-permute-start | bytes 2359304 | tf_op jit(solution)/shard_map/ppermute | solution.py:44
  140.3 5.5 %collective-permute-start.35 = (bf16[256,256]{1,0:T(8,128)(2,1)S(1)}, bf16[256,256]{1,0:T(8,128)(2,1)S(1)}, u32[]{:S(2)}, u32[]{:S(2)}) collective-permute-start(bf16[256,256]{1,0:T(8,128)(2,1)S(1)} %get-tuple-element.38), channel_id=1, source_target_pairs={{0,8},{2,10},{4,12},{6,14},{8,0},{10,2},{12,4},{14,6},{16,24},{18,... | collective-permute-start | bytes 393224 | tf_op jit(solution)/shard_map/ppermute | solution.py:44
  142.3 36.2 %collective-permute-start.46 = (bf16[1024,256]{1,0:T(8,128)(2,1)S(1)}, bf16[1024,256]{1,0:T(8,128)(2,1)S(1)}, u32[]{:S(2)}, u32[]{:S(2)}) collective-permute-start(bf16[1024,256]{1,0:T(8,128)(2,1)S(1)} %choose.11.refs_14_), channel_id=1, source_target_pairs={{0,4},{2,6},{4,0},{6,2},{8,12},{10,14},{12,8},{14,10},{16,20},{18,... | collective-permute-start | bytes 1572872 | tf_op jit(solution)/shard_map/ppermute | solution.py:44
  145.8 9.3 %collective-permute-start.5 = (bf16[128,1536]{1,0:T(8,128)(2,1)}, bf16[128,1536]{1,0:T(8,128)(2,1)}, u32[]{:S(2)}, u32[]{:S(2)}) collective-permute-start(bf16[128,1536]{1,0:T(8,128)(2,1)} %collective-permute-done.4.refs_1_), channel_id=1, source_target_pairs={{0,8},{2,10},{4,12},{6,14},{8,0},{10,2},{12,4},{14,6},{16,24},{18,... | collective-permute-start | bytes 1179656 | tf_op jit(solution)/shard_map/ppermute | solution.py:44
  155.1 50.5 %collective-permute-start.39 = (bf16[1024,128]{1,0:T(8,128)(2,1)}, bf16[1024,128]{1,0:T(8,128)(2,1)S(1)}, u32[]{:S(2)}, u32[]{:S(2)}) collective-permute-start(bf16[1024,128]{1,0:T(8,128)(2,1)} %collective-permute-done.38.refs_10_), channel_id=1, source_target_pairs={{0,8},{2,10},{4,12},{6,14},{8,0},{10,2},{12,4},{14,6},{16,24},{18,... | collective-permute-start | bytes 786440 | tf_op jit(solution)/shard_map/ppermute | solution.py:44
  178.5 27.2 %collective-permute-start.47 = (bf16[1024,256]{1,0:T(8,128)(2,1)S(1)}, bf16[1024,256]{1,0:T(8,128)(2,1)}, u32[]{:S(2)}, u32[]{:S(2)}) collective-permute-start(bf16[1024,256]{1,0:T(8,128)(2,1)S(1)} %choose.11.refs_14_), channel_id=1, source_target_pairs={{0,2},{2,0},{4,6},{6,4},{8,10},{10,8},{12,14},{14,12},{16,18},{18,... | collective-permute-start | bytes 1572872 | tf_op jit(solution)/shard_map/ppermute | solution.py:44
  178.5 27.2 %collective-permute-start.41 = (bf16[1024,256]{1,0:T(8,128)(2,1)}, bf16[1024,256]{1,0:T(8,128)(2,1)S(1)}, u32[]{:S(2)}, u32[]{:S(2)}) collective-permute-start(bf16[1024,256]{1,0:T(8,128)(2,1)} %collective-permute-done.40.refs_12_), channel_id=1, source_target_pairs={{0,4},{2,6},{4,0},{6,2},{8,12},{10,14},{12,8},{14,10},{16,20},{18,... | collective-permute-start | bytes 1572872 | tf_op jit(solution)/shard_map/ppermute | solution.py:44
  179.2 26.5 %collective-permute-start.48 = (bf16[1024,256]{1,0:T(8,128)(2,1)S(1)}, bf16[1024,256]{1,0:T(8,128)(2,1)}, u32[]{:S(2)}, u32[]{:S(2)}) collective-permute-start(bf16[1024,256]{1,0:T(8,128)(2,1)S(1)} %collective-permute-done.46.refs_15_), channel_id=1, source_target_pairs={{0,2},{2,0},{4,6},{6,4},{8,10},{10,8},{12,14},{14,12},{16,18},{18,... | collective-permute-start | bytes 1572872 | tf_op jit(solution)/shard_map/ppermute | solution.py:44
  180.6 24.2 %collective-permute-start.36 = (bf16[256,256]{1,0:T(8,128)(2,1)S(1)}, bf16[256,256]{1,0:T(8,128)(2,1)S(1)}, u32[]{:S(2)}, u32[]{:S(2)}) collective-permute-start(bf16[256,256]{1,0:T(8,128)(2,1)S(1)} %get-tuple-element.40), channel_id=1, source_target_pairs={{0,16},{2,18},{4,20},{6,22},{8,24},{10,26},{12,28},{14,30},{16,0},... | collective-permute-start | bytes 393224 | tf_op jit(solution)/shard_map/ppermute | solution.py:44
  215.5 7.9 %collective-permute-start.49 = (bf16[512,2048]{1,0:T(8,128)(2,1)}, bf16[512,2048]{1,0:T(8,128)(2,1)S(1)}, u32[]{:S(2)}, u32[]{:S(2)}) collective-permute-start(bf16[512,2048]{1,0:T(8,128)(2,1)} %finish.3), channel_id=1, source_target_pairs={{0,1},{1,0},{2,3},{3,2},{4,5},{5,4},{6,7},{7,6},{8,9},{9,8},{10,11... | collective-permute-start | bytes 6291464 | tf_op jit(solution)/shard_map/ppermute | solution.py:44
  (37 other events, 541.4 us)
